TPU v7x, 32 devices: a whole 2x2x4 slice. The times are simulated.
32 devices in a mesh: sp: 16 (over z, y, x), tp: 2 (over core).
Axes of the slice: x: 2, y: 2, z: 4, core: 2. Of those that a mesh axis runs over, the one named last changes fastest.
Arguments:
- latent: bfloat16 [12288, 2048], P(('sp', 'tp')), may hold values from -6 to 6
- condition: float32 [2048], P('sp'), may hold values from -6 to 6
- context_condition: float32 [2048], P('sp'), may hold values from -6 to 6
- context: bfloat16 [1024, 2048], P('sp'), may hold values from -6 to 6
- norm_gain: float32 [2048], replicated, may hold values from 0.1 to 1.9
- shift_weight: bfloat16 [2048, 2048], P('sp', 'tp'), may hold values from -0.1875 to 0.1875
- scale_weight: bfloat16 [2048, 2048], P('sp', 'tp'), may hold values from -0.1875 to 0.1875
- gate_weight: bfloat16 [2048, 2048], P('sp', 'tp'), may hold values from -0.1875 to 0.1875
- query_weight: bfloat16 [2048, 2048], P(None, 'tp'), may hold values from -2 to 2
- key_matrix: bfloat16 [2048, 1024], P(None, 'tp'), may hold values from -2 to 2
- value_matrix: bfloat16 [2048, 1024], P(None, 'tp'), may hold values from -0.125 to 0.125
- sink_logit_head: float32 [16], P('tp'), may hold values from 6 to 10
- out_weight: bfloat16 [2048, 2048], P('tp'), may hold values from -0.125 to 0.125
Outputs:
- updated: bfloat16 [12288, 2048], P(('sp', 'tp'))
All inputs are finite; a program needn't handle non-finite values.
Results may differ from a plain program's by a relative error of at most 0.012.
The roundings to bfloat16 on the way count: a program that leaves them out, or rounds other values in their place, can miss the bound.
Values may be sent and summed in bfloat16 or wider, within the bound.
A program may use at most 128 MiB of HBM per device.

v0:
```python
import functools

import jax
import jax.numpy as jnp
import numpy as np
from jax import lax
from jax.experimental import pallas as pl
from jax.experimental.pallas import tpu as pltpu
from jax.sharding import PartitionSpec as P

QUERY_HEADS = 16
KEY_VALUE_HEADS = 8
HEAD_DIM = 128
WINDOW_REACH = 128
GRID_W = 64
NORM_EPS = 1e-05
MASKED_SCORE = -1e30
LANES = 128
QUAD = 4
MESH = pl.DeviceIdType.MESH
F32 = jnp.float32
BF16 = jnp.bfloat16


def tile_of(extent, most):
    tile = min(extent, most)
    while extent % tile:
        tile -= LANES
    return tile


def block_kernel(
    n_sp,
    n_tp,
    cond_ref,
    ctx_cond_ref,
    gain_ref,
    row_cos,
    row_sin,
    col_cos,
    col_sin,
    sink_ref,
    latent_hbm,
    context_hbm,
    shift_hbm,
    scale_hbm,
    gate_hbm,
    wq_hbm,
    wk_hbm,
    wv_hbm,
    wo_hbm,
    out_ref,
    latent,
    context,
    shift_w,
    scale_w,
    gate_w,
    wq,
    wk,
    wv,
    wo,
    part,
    gathered,
    full,
    mod,
    hidden,
    ctx_hidden,
    queries,
    kv,
    ctx_kv,
    attended,
    partial_out,
    partial_in,
    own_total,
    cos_ref,
    sin_ref,
    halo_raw,
    load_sem,
    rs_send,
    rs_recv,
    ag_send,
    ag_recv,
    tp_send,
    tp_recv,
    hid_send,
    hid_recv,
    ctx_send,
    ctx_recv,
    halo_send,
    halo_recv,
    edge_send,
    edge_recv,
    out_send,
    out_recv,
):
    sp = lax.axis_index("sp")
    tp = lax.axis_index("tp")
    rows, width = latent.shape
    group_rows = rows * n_tp
    columns = shift_w.shape[1]
    chunks = columns // LANES
    per = part.shape[1]
    query_width = wq.shape[1]
    pair = wk.shape[1]
    kv_local = pair // HEAD_DIM
    per_group = query_width // pair
    ctx_rows = context.shape[0]

    loads = [
        pltpu.make_async_copy(src, dst, load_sem.at[i])
        for i, (src, dst) in enumerate(
            [
                (shift_hbm, shift_w),
                (scale_hbm, scale_w),
                (gate_hbm, gate_w),
                (context_hbm, context),
                (latent_hbm, latent),
                (wk_hbm, wk),
                (wv_hbm, wv),
                (wq_hbm, wq),
                (wo_hbm, wo),
            ]
        )
    ]
    for load in loads:
        load.start()

    barrier = pltpu.get_barrier_semaphore()

    def greet_sp(d, carry):
        pl.semaphore_signal(
            barrier, inc=1, device_id={"sp": lax.rem(sp + d, n_sp)}, device_id_type=MESH
        )
        return carry

    def greet_tp(d, carry):
        pl.semaphore_signal(
            barrier, inc=1, device_id={"tp": lax.rem(tp + d, n_tp)}, device_id_type=MESH
        )
        return carry

    lax.fori_loop(1, n_sp, greet_sp, 0)
    lax.fori_loop(1, n_tp, greet_tp, 0)

    def silu(v):
        return v / (1.0 + jnp.exp(-v))

    depth = cond_ref.shape[1]
    row_id = lax.broadcasted_iota(jnp.int32, (16, depth), 0)
    active = jnp.where(
        row_id == 0,
        jnp.broadcast_to(silu(cond_ref[...]), (16, depth)),
        jnp.broadcast_to(silu(ctx_cond_ref[...]), (16, depth)),
    ).astype(BF16)
    part[...] = jnp.zeros_like(part)
    vector = 0
    for load, weight, count in zip(loads[:3], (shift_w, scale_w, gate_w), (2, 2, 1)):
        load.wait()
        product = jnp.dot(active, weight[...], preferred_element_type=F32)
        for v in range(count):
            for j in range(chunks):
                g = vector * chunks + j
                part[g // per, g % per : g % per + 1, :] = product[
                    v : v + 1, j * LANES : (j + 1) * LANES
                ]
            vector += 1

    pl.semaphore_wait(barrier, n_sp + n_tp - 2)

    def rs_copy(d):
        peer = lax.rem(sp + d, n_sp)
        return pltpu.make_async_remote_copy(
            src_ref=part.at[peer],
            dst_ref=gathered.at[sp],
            send_sem=rs_send.at[peer],
            recv_sem=rs_recv.at[sp],
            device_id={"sp": peer},
            device_id_type=MESH,
        )

    def rs_arrival(d):
        peer = lax.rem(sp + d, n_sp)
        return pltpu.make_async_remote_copy(
            src_ref=part.at[peer],
            dst_ref=gathered.at[peer],
            send_sem=rs_send.at[peer],
            recv_sem=rs_recv.at[peer],
            device_id={"sp": peer},
            device_id_type=MESH,
        )

    def loop(low, high, f):
        def step(i, carry):
            f(i)
            return carry

        lax.fori_loop(low, high, step, 0)

    loop(1, n_sp, lambda d: rs_copy(d).start())
    gathered[sp] = part[sp]

    grid_rows = group_rows // GRID_W
    grid_pad = WINDOW_REACH // GRID_W
    in_row = lax.broadcasted_iota(jnp.int32, (GRID_W, HEAD_DIM), 1) < HEAD_DIM // 2

    def fill_angles(i):
        row = jnp.clip(sp * grid_rows - grid_pad + i, 0, n_sp * grid_rows - 1)
        at = pl.ds(pl.multiple_of(i * GRID_W, GRID_W), GRID_W)
        for target, by_row, by_col in ((cos_ref, row_cos, col_cos), (sin_ref, row_sin, col_sin)):
            spread = jnp.broadcast_to(by_row[pl.ds(row, 1), :], (GRID_W, HEAD_DIM))
            target[at, :] = jnp.where(in_row, spread, by_col[...])

    loop(0, grid_rows + 2 * grid_pad, fill_angles)
    loop(1, n_sp, lambda d: rs_arrival(d).wait_recv())
    full[tp, sp] = jnp.sum(gathered[...], axis=0)

    def ag_copy(d):
        peer = lax.rem(sp + d, n_sp)
        return pltpu.make_async_remote_copy(
            src_ref=full.at[tp, sp],
            dst_ref=full.at[tp, sp],
            send_sem=ag_send.at[peer],
            recv_sem=ag_recv.at[sp],
            device_id={"sp": peer},
            device_id_type=MESH,
        )

    def ag_arrival(d):
        peer = lax.rem(sp + d, n_sp)
        return pltpu.make_async_remote_copy(
            src_ref=full.at[tp, sp],
            dst_ref=full.at[tp, peer],
            send_sem=ag_send.at[peer],
            recv_sem=ag_recv.at[peer],
            device_id={"sp": peer},
            device_id_type=MESH,
        )

    loop(1, n_sp, lambda d: ag_copy(d).start())

    raw_halo = rows >= WINDOW_REACH
    has_next, has_last = sp < n_sp - 1, sp > 0
    holds_last, holds_first = tp == n_tp - 1, tp == 0

    def raw_copy(up):
        which = 0 if up else 1
        return pltpu.make_async_remote_copy(
            src_ref=latent.at[pl.ds(rows - WINDOW_REACH if up else 0, WINDOW_REACH)],
            dst_ref=halo_raw.at[which],
            send_sem=halo_send.at[which],
            recv_sem=halo_recv.at[which],
            device_id={"sp": lax.rem(sp + (1 if up else n_sp - 1), n_sp)},
            device_id_type=MESH,
        )

    loads[4].wait()
    if raw_halo:

        @pl.when(has_next & holds_last)
        def _():
            raw_copy(True).start()

        @pl.when(has_last & holds_first)
        def _():
            raw_copy(False).start()

    loop(1, n_sp, lambda d: ag_arrival(d).wait_recv())

    def tp_copy(d, mine):
        peer = lax.rem(tp + d, n_tp)
        slot = tp if mine else peer
        return pltpu.make_async_remote_copy(
            src_ref=full.at[tp],
            dst_ref=full.at[slot],
            send_sem=tp_send.at[peer],
            recv_sem=tp_recv.at[slot],
            device_id={"tp": peer},
            device_id_type=MESH,
        )

    loop(1, n_tp, lambda d: tp_copy(d, True).start())
    loop(1, n_tp, lambda d: tp_copy(d, False).wait_recv())
    for t in range(n_tp):
        for v in range(5):
            for j in range(chunks):
                g = v * chunks + j
                column = t * columns + j * LANES
                mod[v : v + 1, column : column + LANES] = full[t, g // per, g % per : g % per + 1, :]
    gain = gain_ref[...]
    mod[2:3, :] = gain * (1.0 + mod[2:3, :])
    mod[3:4, :] = gain * (1.0 + mod[3:4, :])

    def normed(block, shift_row, scale_row):
        floats = block.astype(F32)
        inverse = lax.rsqrt(jnp.mean(floats * floats, axis=-1, keepdims=True) + NORM_EPS)
        return (
            floats * inverse * mod[scale_row : scale_row + 1, :] + mod[shift_row : shift_row + 1, :]
        ).astype(BF16)

    for i in (3, 5, 6):
        loads[i].wait()
    ctx_hidden[...] = normed(context[...], 1, 3)
    tile = tile_of(pair, 512)

    def ctx_project(j):
        at = pl.multiple_of(j * tile, tile)
        ctx_kv[sp, :, pl.ds(at, tile)] = jnp.dot(
            ctx_hidden[...], wk[:, pl.ds(at, tile)], preferred_element_type=F32
        ).astype(BF16)
        ctx_kv[sp, :, pl.ds(pl.multiple_of(pair + at, tile), tile)] = jnp.dot(
            ctx_hidden[...], wv[:, pl.ds(at, tile)], preferred_element_type=F32
        ).astype(BF16)

    loop(0, pair // tile, ctx_project)

    lines = n_sp // QUAD
    line, corner = sp // QUAD, lax.rem(sp, QUAD)

    across = corner + 1 - 2 * lax.rem(corner, 2)
    beside = lax.rem(corner + 2, QUAD)
    opposite = QUAD - 1 - corner

    def ctx_copy(slot, peer, sem, half=None):
        cols = slice(None) if half is None else pl.ds(half * pair, pair)
        return pltpu.make_async_remote_copy(
            src_ref=ctx_kv.at[slot, :, cols],
            dst_ref=ctx_kv.at[slot, :, cols],
            send_sem=ctx_send.at[sem],
            recv_sem=ctx_recv.at[slot, half or 0],
            device_id={"sp": peer},
            device_id_type=MESH,
        )

    ctx_sends = []

    def send_ctx(slot, peer, half=None):
        copy = ctx_copy(slot, peer, len(ctx_sends), half)
        copy.start()
        ctx_sends.append(copy)

    def send_quad(slot):
        send_ctx(slot, line * QUAD + across)
        send_ctx(slot, line * QUAD + beside)

    for d in range(1, lines):
        send_ctx(sp, lax.rem(line + d, lines) * QUAD + corner)
    send_quad(sp)

    def line_base(d):
        return lax.rem(line + lines - d, lines) * QUAD

    def forward(d):
        slot = line_base(d) + corner
        ctx_copy(slot, sp, 0).wait_recv()
        send_quad(slot)

    def relay(d):
        ctx_copy(line_base(d) + across, sp, 0).wait_recv()
        send_ctx(line_base(d) + across, line * QUAD + beside, 0)
        ctx_copy(line_base(d) + beside, sp, 0).wait_recv()
        send_ctx(line_base(d) + beside, line * QUAD + across, 1)

    def serve(step):
        if step < lines:
            if step + 1 < lines:
                forward(step + 1)
            relay(step)

    strip = 32
    own_start = pl.multiple_of(WINDOW_REACH + tp * rows, strip)

    def norm_strip(i):
        at = pl.multiple_of(i * strip, strip)
        hidden[pl.ds(pl.multiple_of(own_start + at, strip), strip), :] = normed(
            latent[pl.ds(at, strip), :], 0, 2
        )

    loop(0, rows // strip, norm_strip)

    def hid_copy(d, mine):
        peer = lax.rem(tp + d, n_tp)
        slot = tp if mine else peer
        at = pl.multiple_of(WINDOW_REACH + slot * rows, strip)
        mine_at = pl.multiple_of(WINDOW_REACH + tp * rows, strip)
        return pltpu.make_async_remote_copy(
            src_ref=hidden.at[pl.ds(mine_at, rows)],
            dst_ref=hidden.at[pl.ds(at, rows)],
            send_sem=hid_send.at[peer],
            recv_sem=hid_recv.at[slot],
            device_id={"tp": peer},
            device_id_type=MESH,
        )

    loop(1, n_tp, lambda d: hid_copy(d, True).start())

    def edge_copy(low, d, mine):
        owner = n_tp - 1 if low else 0
        peer = lax.rem(tp + d, n_tp) if mine else tp
        which = 0 if low else 1
        region = pl.ds(0 if low else WINDOW_REACH + group_rows, WINDOW_REACH)
        return pltpu.make_async_remote_copy(
            src_ref=hidden.at[region],
            dst_ref=hidden.at[region],
            send_sem=edge_send.at[which, peer],
            recv_sem=edge_recv.at[which],
            device_id={"tp": peer},
            device_id_type=MESH,
        )

    def receive_edge(low):
        which = 0 if low else 1
        base = 0 if low else WINDOW_REACH + group_rows
        raw_copy(low).wait_recv()

        def one(i):
            at = pl.multiple_of(i * strip, strip)
            hidden[pl.ds(pl.multiple_of(base + at, strip), strip), :] = normed(
                halo_raw[which, pl.ds(at, strip), :], 0, 2
            )

        loop(0, WINDOW_REACH // strip, one)
        loop(1, n_tp, lambda d: edge_copy(low, d, True).start())

    if raw_halo:

        @pl.when(has_last & holds_last)
        def _():
            receive_edge(True)

        @pl.when(has_next & holds_first)
        def _():
            receive_edge(False)

        @pl.when(jnp.logical_not(has_last))
        def _():
            hidden[0:WINDOW_REACH, :] = jnp.zeros((WINDOW_REACH, width), BF16)

        @pl.when(jnp.logical_not(has_next))
        def _():
            hidden[WINDOW_REACH + group_rows :, :] = jnp.zeros((WINDOW_REACH, width), BF16)

    quarter = HEAD_DIM // 4
    def turned(values, cosine, sine):
        pieces = []
        lane = lax.broadcasted_iota(jnp.int32, cosine.shape, 1)
        low_half = lax.rem(lane, 2 * quarter) < quarter
        for h in range(values.shape[1] // HEAD_DIM):
            u = values[:, h * HEAD_DIM : (h + 1) * HEAD_DIM]
            other = jnp.where(
                low_half, pltpu.roll(u, HEAD_DIM - quarter, 1), pltpu.roll(u, quarter, 1)
            )
            pieces.append(u * cosine + other * sine)
        return jnp.concatenate(pieces, axis=1).astype(BF16)

    def project_kv(start, count):
        source = pl.ds(pl.multiple_of(start, strip), count)

        def one(j):
            col = pl.multiple_of(j * tile, tile)
            keys = jnp.dot(hidden[source, :], wk[:, pl.ds(col, tile)], preferred_element_type=F32)
            kv[source, pl.ds(col, tile)] = turned(keys, cos_ref[source, :], sin_ref[source, :])
            values = jnp.dot(hidden[source, :], wv[:, pl.ds(col, tile)], preferred_element_type=F32)
            kv[source, pl.ds(pl.multiple_of(pair + col, tile), tile)] = values.astype(BF16)

        loop(0, pair // tile, one)

    def project_q(slot):
        target = pl.ds(pl.multiple_of(slot * rows, strip), rows)
        source = pl.ds(pl.multiple_of(WINDOW_REACH + slot * rows, strip), rows)
        q_tile = tile_of(query_width, 512)

        def one(j):
            col = pl.multiple_of(j * q_tile, q_tile)
            q = jnp.dot(hidden[source, :], wq[:, pl.ds(col, q_tile)], preferred_element_type=F32)
            queries[target, pl.ds(col, q_tile)] = turned(
                q * factor, cos_ref[source, :], sin_ref[source, :]
            )

        loop(0, query_width // q_tile, one)

    log2e = 1.4426950408889634
    factor = HEAD_DIM ** (-0.5) * log2e
    project_kv(WINDOW_REACH + tp * rows, rows)
    serve(0)
    loop(1, n_tp, lambda d: hid_copy(d, False).wait_recv())
    loop(1, n_tp, lambda d: project_kv(WINDOW_REACH + lax.rem(tp + d, n_tp) * rows, rows))
    serve(1)

    def halo_copy(up):
        source = group_rows if up else WINDOW_REACH
        target = 0 if up else group_rows + WINDOW_REACH
        which = 0 if up else 1
        return pltpu.make_async_remote_copy(
            src_ref=kv.at[pl.ds(source, WINDOW_REACH)],
            dst_ref=kv.at[pl.ds(target, WINDOW_REACH)],
            send_sem=halo_send.at[which],
            recv_sem=halo_recv.at[which],
            device_id={"sp": lax.rem(sp + (1 if up else n_sp - 1), n_sp)},
            device_id_type=MESH,
        )

    if not raw_halo:

        @pl.when(has_next)
        def _():
            halo_copy(True).start()

        @pl.when(has_last)
        def _():
            halo_copy(False).start()

        @pl.when(jnp.logical_not(has_last))
        def _():
            kv[0:WINDOW_REACH, :] = jnp.zeros((WINDOW_REACH, 2 * pair), BF16)

        @pl.when(jnp.logical_not(has_next))
        def _():
            kv[group_rows + WINDOW_REACH :, :] = jnp.zeros((WINDOW_REACH, 2 * pair), BF16)

    loads[7].wait()
    project_q(tp)
    serve(2)
    loop(1, n_tp, lambda d: project_q(lax.rem(tp + d, n_tp)))
    for step in range(3, lines):
        serve(step)
    if raw_halo:

        @pl.when(has_last & jnp.logical_not(holds_last))
        def _():
            edge_copy(True, 0, False).wait_recv()

        @pl.when(has_next & jnp.logical_not(holds_first))
        def _():
            edge_copy(False, 0, False).wait_recv()

        project_kv(0, WINDOW_REACH)
        project_kv(WINDOW_REACH + group_rows, WINDOW_REACH)
    else:

        @pl.when(has_last)
        def _():
            halo_copy(True).wait_recv()

        @pl.when(has_next)
        def _():
            halo_copy(False).wait_recv()

    def opposite_arrivals(i):
        slot = i * QUAD + opposite
        ctx_copy(slot, sp, 0, 0).wait_recv()
        ctx_copy(slot, sp, 0, 1).wait_recv()

    loop(0, lines, opposite_arrivals)

    span = 3 * WINDOW_REACH
    stacked = per_group * WINDOW_REACH
    total_rows = group_rows * n_sp
    ctx_total = n_sp * ctx_rows
    contract = (((1,), (1,)), ((), ()))

    def attend(block):
        begin = pl.multiple_of(block * WINDOW_REACH, WINDOW_REACH)
        here = pl.ds(begin, WINDOW_REACH)
        around = pl.ds(begin, span)
        query_at = lax.rem(
            lax.broadcasted_iota(jnp.int32, (stacked, span), 0), WINDOW_REACH
        ) + WINDOW_REACH
        key_at = lax.broadcasted_iota(jnp.int32, (stacked, span), 1)
        key_pos = sp * group_rows + begin - WINDOW_REACH + key_at
        allowed = (
            (jnp.abs(key_at - query_at) <= WINDOW_REACH) & (key_pos >= 0) & (key_pos < total_rows)
        )
        for h in range(kv_local):
            heads = [h * per_group + i for i in range(per_group)]
            cols = slice(h * HEAD_DIM, (h + 1) * HEAD_DIM)
            value_cols = slice(pair + h * HEAD_DIM, pair + (h + 1) * HEAD_DIM)
            q = jnp.concatenate(
                [queries[here, i * HEAD_DIM : (i + 1) * HEAD_DIM] for i in heads], axis=0
            )
            band = lax.dot_general(q, kv[around, cols], contract, preferred_element_type=F32)
            band = jnp.where(allowed, band, MASKED_SCORE)
            ctx_keys = ctx_kv[:, :, cols].reshape(ctx_total, HEAD_DIM)
            ctx_values = ctx_kv[:, :, value_cols].reshape(ctx_total, HEAD_DIM)
            far = lax.dot_general(q, ctx_keys, contract, preferred_element_type=F32)
            sink = jnp.concatenate(
                [jnp.full((WINDOW_REACH, 1), sink_ref[0, i] * log2e, F32) for i in heads], axis=0
            )
            top = jnp.maximum(
                jnp.maximum(
                    jnp.max(band, axis=-1, keepdims=True), jnp.max(far, axis=-1, keepdims=True)
                ),
                sink,
            )
            band_exp = jnp.exp2(band - top)
            far_exp = jnp.exp2(far - top)
            total = (
                jnp.sum(band_exp, axis=-1, keepdims=True)
                + jnp.sum(far_exp, axis=-1, keepdims=True)
                + jnp.exp2(sink - top)
            )
            mixed = jnp.dot(
                band_exp.astype(BF16), kv[around, value_cols], preferred_element_type=F32
            ) + jnp.dot(far_exp.astype(BF16), ctx_values, preferred_element_type=F32)
            mixed = (mixed / total).astype(BF16)
            for n, i in enumerate(heads):
                attended[here, i * HEAD_DIM : (i + 1) * HEAD_DIM] = mixed[
                    n * WINDOW_REACH : (n + 1) * WINDOW_REACH
                ]

    by_part = rows % WINDOW_REACH == 0
    part_blocks = rows // WINDOW_REACH

    def attend_part(slot):
        if by_part:
            loop(0, part_blocks, lambda b: attend(slot * part_blocks + b))

    if not by_part:
        loop(0, group_rows // WINDOW_REACH, attend)
    loads[8].wait()
    out_tile = tile_of(width, 512)

    def out_copy(d, mine):
        peer = lax.rem(tp + d, n_tp)
        slot = tp if mine else peer
        return pltpu.make_async_remote_copy(
            src_ref=partial_out.at[peer],
            dst_ref=partial_in.at[slot],
            send_sem=out_send.at[peer],
            recv_sem=out_recv.at[slot],
            device_id={"tp": peer},
            device_id_type=MESH,
        )

    def project_out(slot, store):
        source = pl.ds(pl.multiple_of(slot * rows, strip), rows)

        def one(j):
            cols = pl.ds(pl.multiple_of(j * out_tile, out_tile), out_tile)
            store(
                cols,
                jnp.dot(attended[source, :], wo[:, cols], preferred_element_type=F32).astype(BF16),
            )

        loop(0, width // out_tile, one)

    def peer_part(d):
        slot = lax.rem(tp + d, n_tp)
        attend_part(slot)

        def store(cols, value):
            partial_out[slot, :, cols] = value

        project_out(slot, store)
        out_copy(d, True).start()

    loop(1, n_tp, peer_part)
    attend_part(tp)

    def keep(cols, value):
        own_total[:, cols] = value.astype(F32)

    project_out(tp, keep)
    loop(1, n_tp, lambda d: out_copy(d, False).wait_recv())

    def finish(i):
        at = pl.ds(pl.multiple_of(i * strip, strip), strip)
        mixed = own_total[at, :]
        for d in range(1, n_tp):
            mixed = mixed + partial_in[lax.rem(tp + d, n_tp), at, :].astype(F32)
        out_ref[at, :] = (latent[at, :].astype(F32) + mod[4:5, :] * mixed).astype(BF16)

    loop(0, rows // strip, finish)

    loop(1, n_sp, lambda d: rs_copy(d).wait_send())
    loop(1, n_sp, lambda d: ag_copy(d).wait_send())
    loop(1, n_tp, lambda d: tp_copy(d, True).wait_send())
    loop(1, n_tp, lambda d: hid_copy(d, True).wait_send())
    loop(1, n_tp, lambda d: out_copy(d, True).wait_send())
    for copy in ctx_sends:
        copy.wait_send()

    if raw_halo:

        @pl.when(has_next & holds_last)
        def _():
            raw_copy(True).wait_send()

        @pl.when(has_last & holds_first)
        def _():
            raw_copy(False).wait_send()

        @pl.when(has_last & holds_last)
        def _():
            loop(1, n_tp, lambda d: edge_copy(True, d, True).wait_send())

        @pl.when(has_next & holds_first)
        def _():
            loop(1, n_tp, lambda d: edge_copy(False, d, True).wait_send())
    else:

        @pl.when(has_next)
        def _():
            halo_copy(True).wait_send()

        @pl.when(has_last)
        def _():
            halo_copy(False).wait_send()


def angle_tables(total_rows):
    inv_freq = np.power(
        10000.0, -np.arange(0, HEAD_DIM // 2, 2, dtype=np.float64) / (HEAD_DIM // 2)
    ).astype(np.float32)

    def tables(count):
        angle = (np.arange(count, dtype=np.float32)[:, None] * inv_freq).astype(np.float64)
        cosine, sine = np.cos(angle), np.sin(angle)
        return (
            np.concatenate([cosine, cosine], axis=1).astype(np.float32),
            np.concatenate([-sine, sine], axis=1).astype(np.float32),
        )

    empty = HEAD_DIM // 2
    by_row = [np.pad(t, ((0, 0), (0, empty))) for t in tables(total_rows // GRID_W)]
    by_col = [np.pad(t, ((0, 0), (empty, 0))) for t in tables(GRID_W)]
    return by_row + by_col


def shards(
    n_sp,
    n_tp,
    latent,
    condition,
    context_condition,
    context,
    norm_gain,
    shift_weight,
    scale_weight,
    gate_weight,
    query_weight,
    key_matrix,
    value_matrix,
    sink_logit_head,
    out_weight,
):
    rows, width = latent.shape
    group_rows = rows * n_tp
    angles = [jnp.asarray(t) for t in angle_tables(group_rows * n_sp)]
    columns = shift_weight.shape[1]
    groups = 5 * columns // LANES
    per = -(-groups // n_sp)
    query_width = query_weight.shape[1]
    pair = key_matrix.shape[1]
    ctx_rows = context.shape[0]
    lines = n_sp // QUAD
    ctx_sends = (lines - 1) + 4 * lines
    dma = pltpu.SemaphoreType.DMA
    vmem = pl.BlockSpec(memory_space=pltpu.VMEM)
    anywhere = pl.BlockSpec(memory_space=pl.ANY)

    def like(array):
        return pltpu.VMEM(array.shape, array.dtype)

    return pl.pallas_call(
        functools.partial(block_kernel, n_sp, n_tp),
        out_shape=jax.ShapeDtypeStruct((rows, width), BF16),
        in_specs=[vmem] * 7 + [pl.BlockSpec(memory_space=pltpu.SMEM)] + [anywhere] * 9,
        out_specs=vmem,
        scratch_shapes=[
            like(latent),
            like(context),
            like(shift_weight),
            like(scale_weight),
            like(gate_weight),
            like(query_weight),
            like(key_matrix),
            like(value_matrix),
            like(out_weight),
            pltpu.VMEM((n_sp, per, LANES), F32),
            pltpu.VMEM((n_sp, per, LANES), F32),
            pltpu.VMEM((n_tp, n_sp, per, LANES), F32),
            pltpu.VMEM((8, width), F32),
            pltpu.VMEM((group_rows + 2 * WINDOW_REACH, width), BF16),
            like(context),
            pltpu.VMEM((group_rows, query_width), BF16),
            pltpu.VMEM((group_rows + 2 * WINDOW_REACH, 2 * pair), BF16),
            pltpu.VMEM((n_sp, ctx_rows, 2 * pair), BF16),
            pltpu.VMEM((group_rows, query_width), BF16),
            pltpu.VMEM((n_tp, rows, width), BF16),
            pltpu.VMEM((n_tp, rows, width), BF16),
            pltpu.VMEM((rows, width), F32),
            pltpu.VMEM((group_rows + 2 * WINDOW_REACH, HEAD_DIM), F32),
            pltpu.VMEM((group_rows + 2 * WINDOW_REACH, HEAD_DIM), F32),
            pltpu.VMEM((2, WINDOW_REACH, width), BF16),
            dma((9,)),
            dma((n_sp,)),
            dma((n_sp,)),
            dma((n_sp,)),
            dma((n_sp,)),
            dma((n_tp,)),
            dma((n_tp,)),
            dma((n_tp,)),
            dma((n_tp,)),
            dma((ctx_sends,)),
            dma((n_sp, 2)),
            dma((2,)),
            dma((2,)),
            dma((2, n_tp)),
            dma((2,)),
            dma((n_tp,)),
            dma((n_tp,)),
        ],
        compiler_params=pltpu.CompilerParams(
            collective_id=0, has_side_effects=True, vmem_limit_bytes=63 * 1024 * 1024
        ),
    )(
        condition.reshape(1, -1),
        context_condition.reshape(1, -1),
        norm_gain.reshape(1, -1),
        *angles,
        sink_logit_head.reshape(1, -1),
        latent,
        context,
        shift_weight,
        scale_weight,
        gate_weight,
        query_weight,
        key_matrix,
        value_matrix,
        out_weight,
    )


def solution(mesh):
    placed = (
        P(("sp", "tp"), None),
        P("sp"),
        P("sp"),
        P("sp", None),
        P(),
        P("sp", "tp"),
        P("sp", "tp"),
        P("sp", "tp"),
        P(None, "tp"),
        P(None, "tp"),
        P(None, "tp"),
        P("tp"),
        P("tp", None),
    )
    return jax.shard_map(
        functools.partial(shards, mesh.shape["sp"], mesh.shape["tp"]),
        mesh=mesh,
        in_specs=placed,
        out_specs=P(("sp", "tp"), None),
        check_vma=False,
    )
```

profile of v0, /device:TPU:0, one launch (start us, length us, event | category | flops | bytes accessed | tf_op | source)
XLA Modules:
  0.0 73.0 jit_solution(4686338014034426280)
XLA Ops:
  0.0 70.3 %shard_map.163 = bf16[384,2048]{1,0:T(8,128)(2,1)} custom-call(f32[1,128]{1,0:T(1,128)} %bitcast.5, f32[1,128]{1,0:T(1,128)} %bitcast.6, f32[1,2048]{1,0:T(1,128)} %bitcast.4, f32[192,128]{1,0:T(8,128)} %constant.8.clone.row_cos, f32[192,128]{1,0:T(8,128)} %constant.9.clone.row_sin, f32[64,128]{1,0:T(8,128)} %constant.10.clone.col_cos, ...), custom_call_target="tpu_custom_call" | custom-call | tf_op jit(solution)/shard_map/pallas_call | solution.py:764
  70.3 2.7 %copy.19 = bf16[384,2048]{1,0:T(8,128)(2,1)} copy(bf16[384,2048]{1,0:T(8,128)(2,1)} %shard_map.163) | data formatting | bytes 3145728
where the time goes:
time: 73.2 us; the launch traced here: 73 us
  Pallas kernels  70.3 us (96%)
  local copies, waits for them, and re-layouts  2.73 us (4%)
    pallas_call x1, Pallas kernels, shards(): pl.pallas_call(functools.partial(block_kernel, n_sp, n_tp), out_shape=jax...  70.3 us
    unnamed x1, local copies, waits for them, and re-layouts  2.73 us

commit v1 on v0

--- a/solution.py
+++ b/solution.py
@@ -80,14 +80,14 @@
     rs_recv,
     ag_send,
     ag_recv,
-    tp_send,
-    tp_recv,
     hid_send,
     hid_recv,
     ctx_send,
     ctx_recv,
     halo_send,
     halo_recv,
+    raw_send,
+    raw_recv,
     edge_send,
     edge_recv,
     out_send,
@@ -127,20 +127,21 @@
 
     barrier = pltpu.get_barrier_semaphore()
 
-    def greet_sp(d, carry):
+    everyone = n_sp * n_tp
+    me = sp * n_tp + tp
+
+    def other(d):
+        at = lax.rem(me + d, everyone)
+        return at // n_tp, lax.rem(at, n_tp)
+
+    def greet(d, carry):
+        peer_sp, peer_tp = other(d)
         pl.semaphore_signal(
-            barrier, inc=1, device_id={"sp": lax.rem(sp + d, n_sp)}, device_id_type=MESH
+            barrier, inc=1, device_id={"sp": peer_sp, "tp": peer_tp}, device_id_type=MESH
         )
         return carry
 
-    def greet_tp(d, carry):
-        pl.semaphore_signal(
-            barrier, inc=1, device_id={"tp": lax.rem(tp + d, n_tp)}, device_id_type=MESH
-        )
-        return carry
-
-    lax.fori_loop(1, n_sp, greet_sp, 0)
-    lax.fori_loop(1, n_tp, greet_tp, 0)
+    lax.fori_loop(1, everyone, greet, 0)
 
     def silu(v):
         return v / (1.0 + jnp.exp(-v))
@@ -165,7 +166,7 @@
                 ]
             vector += 1
 
-    pl.semaphore_wait(barrier, n_sp + n_tp - 2)
+    pl.semaphore_wait(barrier, everyone - 1)
 
     def rs_copy(d):
         peer = lax.rem(sp + d, n_sp)
@@ -196,8 +197,48 @@
 
         lax.fori_loop(low, high, step, 0)
 
+    raw_halo = rows >= WINDOW_REACH
+    has_next, has_last = sp < n_sp - 1, sp > 0
+    holds_last, holds_first = tp == n_tp - 1, tp == 0
+    half_reach = WINDOW_REACH // 2
+
+    def raw_copy(up, half):
+        which = 0 if up else 1
+        base = rows - WINDOW_REACH if up else 0
+        return pltpu.make_async_remote_copy(
+            src_ref=latent.at[pl.ds(base + half * half_reach, half_reach)],
+            dst_ref=halo_raw.at[which, pl.ds(half * half_reach, half_reach)],
+            send_sem=raw_send.at[which, half],
+            recv_sem=raw_recv.at[which, half],
+            device_id={"sp": lax.rem(sp + (1 if up else n_sp - 1), n_sp)},
+            device_id_type=MESH,
+        )
+
+    def send_raw(half):
+        if raw_halo:
+
+            @pl.when(has_next & holds_last)
+            def _():
+                raw_copy(True, half).start()
+
+            @pl.when(has_last & holds_first)
+            def _():
+                raw_copy(False, half).start()
+
     loop(1, n_sp, lambda d: rs_copy(d).start())
     gathered[sp] = part[sp]
+    loads[4].wait()
+    send_raw(0)
+
+    strip = 32
+
+    def scale_strip(i):
+        at = pl.multiple_of(i * strip, strip)
+        floats = latent[pl.ds(at, strip), :].astype(F32)
+        inverse = lax.rsqrt(jnp.mean(floats * floats, axis=-1, keepdims=True) + NORM_EPS)
+        own_total[pl.ds(at, strip), :] = floats * inverse
+
+    loop(0, rows // strip, scale_strip)
 
     grid_rows = group_rows // GRID_W
     grid_pad = WINDOW_REACH // GRID_W
@@ -215,71 +256,32 @@
     full[tp, sp] = jnp.sum(gathered[...], axis=0)
 
     def ag_copy(d):
-        peer = lax.rem(sp + d, n_sp)
+        peer_sp, peer_tp = other(d)
         return pltpu.make_async_remote_copy(
             src_ref=full.at[tp, sp],
             dst_ref=full.at[tp, sp],
-            send_sem=ag_send.at[peer],
-            recv_sem=ag_recv.at[sp],
-            device_id={"sp": peer},
+            send_sem=ag_send.at[peer_tp, peer_sp],
+            recv_sem=ag_recv.at[tp, sp],
+            device_id={"sp": peer_sp, "tp": peer_tp},
             device_id_type=MESH,
         )
 
     def ag_arrival(d):
-        peer = lax.rem(sp + d, n_sp)
+        peer_sp, peer_tp = other(d)
         return pltpu.make_async_remote_copy(
             src_ref=full.at[tp, sp],
-            dst_ref=full.at[tp, peer],
-            send_sem=ag_send.at[peer],
-            recv_sem=ag_recv.at[peer],
-            device_id={"sp": peer},
-            device_id_type=MESH,
-        )
-
-    loop(1, n_sp, lambda d: ag_copy(d).start())
-
-    raw_halo = rows >= WINDOW_REACH
-    has_next, has_last = sp < n_sp - 1, sp > 0
-    holds_last, holds_first = tp == n_tp - 1, tp == 0
-
-    def raw_copy(up):
-        which = 0 if up else 1
-        return pltpu.make_async_remote_copy(
-            src_ref=latent.at[pl.ds(rows - WINDOW_REACH if up else 0, WINDOW_REACH)],
-            dst_ref=halo_raw.at[which],
-            send_sem=halo_send.at[which],
-            recv_sem=halo_recv.at[which],
-            device_id={"sp": lax.rem(sp + (1 if up else n_sp - 1), n_sp)},
-            device_id_type=MESH,
-        )
-
-    loads[4].wait()
-    if raw_halo:
-
-        @pl.when(has_next & holds_last)
-        def _():
-            raw_copy(True).start()
-
-        @pl.when(has_last & holds_first)
-        def _():
-            raw_copy(False).start()
-
-    loop(1, n_sp, lambda d: ag_arrival(d).wait_recv())
-
-    def tp_copy(d, mine):
-        peer = lax.rem(tp + d, n_tp)
-        slot = tp if mine else peer
-        return pltpu.make_async_remote_copy(
-            src_ref=full.at[tp],
-            dst_ref=full.at[slot],
-            send_sem=tp_send.at[peer],
-            recv_sem=tp_recv.at[slot],
-            device_id={"tp": peer},
-            device_id_type=MESH,
-        )
-
-    loop(1, n_tp, lambda d: tp_copy(d, True).start())
-    loop(1, n_tp, lambda d: tp_copy(d, False).wait_recv())
+            dst_ref=full.at[peer_tp, peer_sp],
+            send_sem=ag_send.at[peer_tp, peer_sp],
+            recv_sem=ag_recv.at[peer_tp, peer_sp],
+            device_id={"sp": peer_sp, "tp": peer_tp},
+            device_id_type=MESH,
+        )
+
+    loop(1, everyone, lambda d: ag_copy(d).start())
+    send_raw(1)
+
+    loop(1, everyone, lambda d: ag_arrival(d).wait_recv())
+
     for t in range(n_tp):
         for v in range(5):
             for j in range(chunks):
@@ -366,14 +368,13 @@
                 forward(step + 1)
             relay(step)
 
-    strip = 32
     own_start = pl.multiple_of(WINDOW_REACH + tp * rows, strip)
 
     def norm_strip(i):
         at = pl.multiple_of(i * strip, strip)
-        hidden[pl.ds(pl.multiple_of(own_start + at, strip), strip), :] = normed(
-            latent[pl.ds(at, strip), :], 0, 2
-        )
+        hidden[pl.ds(pl.multiple_of(own_start + at, strip), strip), :] = (
+            own_total[pl.ds(at, strip), :] * mod[2:3, :] + mod[0:1, :]
+        ).astype(BF16)
 
     loop(0, rows // strip, norm_strip)
 
@@ -410,7 +411,8 @@
     def receive_edge(low):
         which = 0 if low else 1
         base = 0 if low else WINDOW_REACH + group_rows
-        raw_copy(low).wait_recv()
+        raw_copy(low, 0).wait_recv()
+        raw_copy(low, 1).wait_recv()
 
         def one(i):
             at = pl.multiple_of(i * strip, strip)
@@ -420,24 +422,6 @@
 
         loop(0, WINDOW_REACH // strip, one)
         loop(1, n_tp, lambda d: edge_copy(low, d, True).start())
-
-    if raw_halo:
-
-        @pl.when(has_last & holds_last)
-        def _():
-            receive_edge(True)
-
-        @pl.when(has_next & holds_first)
-        def _():
-            receive_edge(False)
-
-        @pl.when(jnp.logical_not(has_last))
-        def _():
-            hidden[0:WINDOW_REACH, :] = jnp.zeros((WINDOW_REACH, width), BF16)
-
-        @pl.when(jnp.logical_not(has_next))
-        def _():
-            hidden[WINDOW_REACH + group_rows :, :] = jnp.zeros((WINDOW_REACH, width), BF16)
 
     quarter = HEAD_DIM // 4
     def turned(values, cosine, sine):
@@ -521,6 +505,24 @@
     project_q(tp)
     serve(2)
     loop(1, n_tp, lambda d: project_q(lax.rem(tp + d, n_tp)))
+    if raw_halo:
+
+        @pl.when(has_last & holds_last)
+        def _():
+            receive_edge(True)
+
+        @pl.when(has_next & holds_first)
+        def _():
+            receive_edge(False)
+
+        @pl.when(jnp.logical_not(has_last))
+        def _():
+            hidden[0:WINDOW_REACH, :] = jnp.zeros((WINDOW_REACH, width), BF16)
+
+        @pl.when(jnp.logical_not(has_next))
+        def _():
+            hidden[WINDOW_REACH + group_rows :, :] = jnp.zeros((WINDOW_REACH, width), BF16)
+
     for step in range(3, lines):
         serve(step)
     if raw_halo:
@@ -672,8 +674,7 @@
     loop(0, rows // strip, finish)
 
     loop(1, n_sp, lambda d: rs_copy(d).wait_send())
-    loop(1, n_sp, lambda d: ag_copy(d).wait_send())
-    loop(1, n_tp, lambda d: tp_copy(d, True).wait_send())
+    loop(1, everyone, lambda d: ag_copy(d).wait_send())
     loop(1, n_tp, lambda d: hid_copy(d, True).wait_send())
     loop(1, n_tp, lambda d: out_copy(d, True).wait_send())
     for copy in ctx_sends:
@@ -683,11 +684,13 @@
 
         @pl.when(has_next & holds_last)
         def _():
-            raw_copy(True).wait_send()
+            raw_copy(True, 0).wait_send()
+            raw_copy(True, 1).wait_send()
 
         @pl.when(has_last & holds_first)
         def _():
-            raw_copy(False).wait_send()
+            raw_copy(False, 0).wait_send()
+            raw_copy(False, 1).wait_send()
 
         @pl.when(has_last & holds_last)
         def _():
@@ -795,16 +798,16 @@
             dma((9,)),
             dma((n_sp,)),
             dma((n_sp,)),
-            dma((n_sp,)),
-            dma((n_sp,)),
-            dma((n_tp,)),
-            dma((n_tp,)),
+            dma((n_tp, n_sp)),
+            dma((n_tp, n_sp)),
             dma((n_tp,)),
             dma((n_tp,)),
             dma((ctx_sends,)),
             dma((n_sp, 2)),
             dma((2,)),
             dma((2,)),
+            dma((2, 2)),
+            dma((2, 2)),
             dma((2, n_tp)),
             dma((2,)),
             dma((n_tp,)),

time: 73.2 us -> 76.3 us (1.042)
  the two profiles are of different devices: /device:TPU:0 before, /device:TPU:16 now
where the time goes in v1:
time: 76.3 us; the launch traced here: 76.2 us
  Pallas kernels  73.4 us (96%)
  local copies, waits for them, and re-layouts  2.73 us (4%)
    pallas_call x1, Pallas kernels, shards(): pl.pallas_call(functools.partial(block_kernel, n_sp, n_tp), out_shape=jax...  73.4 us
    unnamed x1, local copies, waits for them, and re-layouts  2.73 us

profile of v1, /device:TPU:16, one launch (start us, length us, event | category | flops | bytes accessed | tf_op | source)
XLA Modules:
  0.0 76.2 jit_solution(5218142203369574062)
XLA Ops:
  0.0 73.4 %shard_map.163 = bf16[384,2048]{1,0:T(8,128)(2,1)} custom-call(f32[1,128]{1,0:T(1,128)} %bitcast.5, f32[1,128]{1,0:T(1,128)} %bitcast.6, f32[1,2048]{1,0:T(1,128)} %bitcast.4, f32[192,128]{1,0:T(8,128)} %constant.8.clone.row_cos, f32[192,128]{1,0:T(8,128)} %constant.9.clone.row_sin, f32[64,128]{1,0:T(8,128)} %constant.10.clone.col_cos, ...), custom_call_target="tpu_custom_call" | custom-call | tf_op jit(solution)/shard_map/pallas_call | solution.py:767
  73.4 2.7 %copy.19 = bf16[384,2048]{1,0:T(8,128)(2,1)} copy(bf16[384,2048]{1,0:T(8,128)(2,1)} %shard_map.163) | data formatting | bytes 3145728

commit v2 on v1

--- a/solution.py
+++ b/solution.py
@@ -66,15 +66,19 @@
     hidden,
     ctx_hidden,
     queries,
-    kv,
+    keys_kept,
+    values_kept,
+    values_t,
     ctx_kv,
+    ctx_values_t,
+    sums,
+    tops,
     attended,
     partial_out,
     partial_in,
     own_total,
     cos_ref,
     sin_ref,
-    halo_raw,
     load_sem,
     rs_send,
     rs_recv,
@@ -86,10 +90,6 @@
     ctx_recv,
     halo_send,
     halo_recv,
-    raw_send,
-    raw_recv,
-    edge_send,
-    edge_recv,
     out_send,
     out_recv,
 ):
@@ -197,38 +197,11 @@
 
         lax.fori_loop(low, high, step, 0)
 
-    raw_halo = rows >= WINDOW_REACH
     has_next, has_last = sp < n_sp - 1, sp > 0
-    holds_last, holds_first = tp == n_tp - 1, tp == 0
-    half_reach = WINDOW_REACH // 2
-
-    def raw_copy(up, half):
-        which = 0 if up else 1
-        base = rows - WINDOW_REACH if up else 0
-        return pltpu.make_async_remote_copy(
-            src_ref=latent.at[pl.ds(base + half * half_reach, half_reach)],
-            dst_ref=halo_raw.at[which, pl.ds(half * half_reach, half_reach)],
-            send_sem=raw_send.at[which, half],
-            recv_sem=raw_recv.at[which, half],
-            device_id={"sp": lax.rem(sp + (1 if up else n_sp - 1), n_sp)},
-            device_id_type=MESH,
-        )
-
-    def send_raw(half):
-        if raw_halo:
-
-            @pl.when(has_next & holds_last)
-            def _():
-                raw_copy(True, half).start()
-
-            @pl.when(has_last & holds_first)
-            def _():
-                raw_copy(False, half).start()
 
     loop(1, n_sp, lambda d: rs_copy(d).start())
     gathered[sp] = part[sp]
     loads[4].wait()
-    send_raw(0)
 
     strip = 32
 
@@ -278,7 +251,6 @@
         )
 
     loop(1, everyone, lambda d: ag_copy(d).start())
-    send_raw(1)
 
     loop(1, everyone, lambda d: ag_arrival(d).wait_recv())
 
@@ -394,35 +366,6 @@
 
     loop(1, n_tp, lambda d: hid_copy(d, True).start())
 
-    def edge_copy(low, d, mine):
-        owner = n_tp - 1 if low else 0
-        peer = lax.rem(tp + d, n_tp) if mine else tp
-        which = 0 if low else 1
-        region = pl.ds(0 if low else WINDOW_REACH + group_rows, WINDOW_REACH)
-        return pltpu.make_async_remote_copy(
-            src_ref=hidden.at[region],
-            dst_ref=hidden.at[region],
-            send_sem=edge_send.at[which, peer],
-            recv_sem=edge_recv.at[which],
-            device_id={"tp": peer},
-            device_id_type=MESH,
-        )
-
-    def receive_edge(low):
-        which = 0 if low else 1
-        base = 0 if low else WINDOW_REACH + group_rows
-        raw_copy(low, 0).wait_recv()
-        raw_copy(low, 1).wait_recv()
-
-        def one(i):
-            at = pl.multiple_of(i * strip, strip)
-            hidden[pl.ds(pl.multiple_of(base + at, strip), strip), :] = normed(
-                halo_raw[which, pl.ds(at, strip), :], 0, 2
-            )
-
-        loop(0, WINDOW_REACH // strip, one)
-        loop(1, n_tp, lambda d: edge_copy(low, d, True).start())
-
     quarter = HEAD_DIM // 4
     def turned(values, cosine, sine):
         pieces = []
@@ -436,17 +379,32 @@
             pieces.append(u * cosine + other * sine)
         return jnp.concatenate(pieces, axis=1).astype(BF16)
 
-    def project_kv(start, count):
-        source = pl.ds(pl.multiple_of(start, strip), count)
+    aligned = rows % WINDOW_REACH == 0
+
+    def project_kv(start):
+        source = pl.ds(pl.multiple_of(start, strip), rows)
 
         def one(j):
             col = pl.multiple_of(j * tile, tile)
             keys = jnp.dot(hidden[source, :], wk[:, pl.ds(col, tile)], preferred_element_type=F32)
-            kv[source, pl.ds(col, tile)] = turned(keys, cos_ref[source, :], sin_ref[source, :])
+            keys_kept[source, pl.ds(col, tile)] = turned(keys, cos_ref[source, :], sin_ref[source, :])
             values = jnp.dot(hidden[source, :], wv[:, pl.ds(col, tile)], preferred_element_type=F32)
-            kv[source, pl.ds(pl.multiple_of(pair + col, tile), tile)] = values.astype(BF16)
+            if aligned:
+                at = pl.ds(pl.multiple_of(start, WINDOW_REACH), rows)
+                values_t[pl.ds(col, tile), at] = values.astype(BF16).T
+            else:
+                values_kept[source, pl.ds(col, tile)] = values.astype(BF16)
 
         loop(0, pair // tile, one)
+
+    def transpose_values():
+        if not aligned:
+
+            def one(i):
+                at = pl.ds(pl.multiple_of(WINDOW_REACH * (i + 1), WINDOW_REACH), WINDOW_REACH)
+                values_t[:, at] = values_kept[at, :].T
+
+            loop(0, group_rows // WINDOW_REACH, one)
 
     def project_q(slot):
         target = pl.ds(pl.multiple_of(slot * rows, strip), rows)
@@ -464,160 +422,244 @@
 
     log2e = 1.4426950408889634
     factor = HEAD_DIM ** (-0.5) * log2e
-    project_kv(WINDOW_REACH + tp * rows, rows)
-    serve(0)
-    loop(1, n_tp, lambda d: hid_copy(d, False).wait_recv())
-    loop(1, n_tp, lambda d: project_kv(WINDOW_REACH + lax.rem(tp + d, n_tp) * rows, rows))
-    serve(1)
-
-    def halo_copy(up):
+    def halo_copies(up):
         source = group_rows if up else WINDOW_REACH
         target = 0 if up else group_rows + WINDOW_REACH
         which = 0 if up else 1
-        return pltpu.make_async_remote_copy(
-            src_ref=kv.at[pl.ds(source, WINDOW_REACH)],
-            dst_ref=kv.at[pl.ds(target, WINDOW_REACH)],
-            send_sem=halo_send.at[which],
-            recv_sem=halo_recv.at[which],
-            device_id={"sp": lax.rem(sp + (1 if up else n_sp - 1), n_sp)},
-            device_id_type=MESH,
-        )
-
-    if not raw_halo:
-
+        peer = {"sp": lax.rem(sp + (1 if up else n_sp - 1), n_sp)}
+        ends = (
+            (keys_kept.at[pl.ds(source, WINDOW_REACH)], keys_kept.at[pl.ds(target, WINDOW_REACH)]),
+            (
+                values_t.at[:, pl.ds(source, WINDOW_REACH)],
+                values_t.at[:, pl.ds(target, WINDOW_REACH)],
+            ),
+        )
+        return [
+            pltpu.make_async_remote_copy(
+                src_ref=src,
+                dst_ref=dst,
+                send_sem=halo_send.at[which, i],
+                recv_sem=halo_recv.at[which, i],
+                device_id=peer,
+                device_id_type=MESH,
+            )
+            for i, (src, dst) in enumerate(ends)
+        ]
+
+    def send_halo():
         @pl.when(has_next)
         def _():
-            halo_copy(True).start()
+            for copy in halo_copies(True):
+                copy.start()
 
         @pl.when(has_last)
         def _():
-            halo_copy(False).start()
+            for copy in halo_copies(False):
+                copy.start()
+
+        def clear(at):
+            region = pl.ds(at, WINDOW_REACH)
+            keys_kept[region, :] = jnp.zeros((WINDOW_REACH, pair), BF16)
+            values_t[:, region] = jnp.zeros((pair, WINDOW_REACH), BF16)
 
         @pl.when(jnp.logical_not(has_last))
         def _():
-            kv[0:WINDOW_REACH, :] = jnp.zeros((WINDOW_REACH, 2 * pair), BF16)
+            clear(0)
 
         @pl.when(jnp.logical_not(has_next))
         def _():
-            kv[group_rows + WINDOW_REACH :, :] = jnp.zeros((WINDOW_REACH, 2 * pair), BF16)
-
+            clear(group_rows + WINDOW_REACH)
+
+    def receive_halo():
+        @pl.when(has_last)
+        def _():
+            for copy in halo_copies(True):
+                copy.wait_recv()
+
+        @pl.when(has_next)
+        def _():
+            for copy in halo_copies(False):
+                copy.wait_recv()
+
+    span = 3 * WINDOW_REACH
+    stacked = per_group * WINDOW_REACH
+    contract = (((1,), (1,)), ((), ()))
+    blocks = group_rows // WINDOW_REACH
+    lines_each = max(1, 256 // (QUAD * ctx_rows))
+    ctx_chunks = lines // lines_each
+    slots_each = QUAD * lines_each
+    chunk_rows = slots_each * ctx_rows
+    ahead = lax.rem(
+        lax.broadcasted_iota(jnp.int32, (WINDOW_REACH, stacked), 1), WINDOW_REACH
+    ) - lax.broadcasted_iota(jnp.int32, (WINDOW_REACH, stacked), 0)
+    WINDOW = "window"
+
+    def chunk_at(k):
+        return lax.rem(line // lines_each + ctx_chunks - k, ctx_chunks)
+
+    def query_heads(h):
+        return range(h * per_group, (h + 1) * per_group)
+
+    def scores(block, h, piece):
+        begin = pl.multiple_of(block * WINDOW_REACH, WINDOW_REACH)
+        cols = slice(h * HEAD_DIM, (h + 1) * HEAD_DIM)
+        q = jnp.concatenate(
+            [
+                queries[pl.ds(begin, WINDOW_REACH), i * HEAD_DIM : (i + 1) * HEAD_DIM]
+                for i in query_heads(h)
+            ],
+            axis=0,
+        )
+        if piece is not WINDOW:
+            keys = ctx_kv[pl.ds(piece * slots_each, slots_each), :, cols]
+            keys = keys.reshape(chunk_rows, HEAD_DIM)
+            return lax.dot_general(keys, q, contract, preferred_element_type=F32)
+        keys = keys_kept[pl.ds(begin, span), cols]
+        band = lax.dot_general(keys, q, contract, preferred_element_type=F32)
+        lowest = jnp.where((block > 0) | has_last, 0, -span)
+        highest = jnp.where((block < blocks - 1) | has_next, 0, span)
+        return jnp.concatenate(
+            [
+                jnp.where(ahead <= lowest, band[:WINDOW_REACH], MASKED_SCORE),
+                band[WINDOW_REACH : 2 * WINDOW_REACH],
+                jnp.where(ahead >= highest, band[2 * WINDOW_REACH :], MASKED_SCORE),
+            ],
+            axis=0,
+        )
+
+    def weighted(block, h, piece, probs):
+        cols = slice(h * HEAD_DIM, (h + 1) * HEAD_DIM)
+        if piece is WINDOW:
+            begin = pl.multiple_of(block * WINDOW_REACH, WINDOW_REACH)
+            values = values_t[cols, pl.ds(begin, span)]
+        else:
+            begin = pl.multiple_of(piece * chunk_rows, chunk_rows)
+            values = ctx_values_t[cols, pl.ds(begin, chunk_rows)]
+        ones = jnp.ones((16, probs.shape[0]), BF16)
+        return jnp.dot(
+            jnp.concatenate([values, ones], axis=0), probs, preferred_element_type=F32
+        )[: HEAD_DIM + 8]
+
+    def sinks(h):
+        return jnp.concatenate(
+            [jnp.full((1, WINDOW_REACH), sink_ref[0, i] * log2e, F32) for i in query_heads(h)],
+            axis=1,
+        )
+
+    def attend(items, first=False, last=False):
+        tasks = [(b, h, pieces) for b, pieces in items for h in range(kv_local)]
+        top, total = {}, {}
+        following = {i: scores(b, h, pieces[0]) for i, (b, h, pieces) in enumerate(tasks)}
+        for step in range(max(len(pieces) for _, pieces in items)):
+            current, following, now = following, {}, {}
+            live = [(i, *task) for i, task in enumerate(tasks) if step < len(task[2])]
+            for i, b, h, pieces in live:
+                if step + 1 < len(pieces):
+                    following[i] = scores(b, h, pieces[step + 1])
+            for i, b, h, pieces in live:
+                if step == 0:
+                    top[i] = sinks(h) if first else tops[b, h, 0:1, :]
+                now[i] = jnp.maximum(top[i], jnp.max(current[i], axis=0, keepdims=True))
+            probs = {i: jnp.exp2(current[i] - now[i]).astype(BF16) for i, *_ in live}
+            for i, b, h, pieces in live:
+                added = weighted(b, h, pieces[step], probs[i])
+                shrink = jnp.exp2(top[i] - now[i])
+                if step == 0 and first:
+                    total[i] = jnp.concatenate(
+                        [added[:HEAD_DIM], added[HEAD_DIM:] + shrink], axis=0
+                    )
+                else:
+                    total[i] = (sums[b, h] if step == 0 else total[i]) * shrink + added
+                top[i] = now[i]
+        for i, (b, h, pieces) in enumerate(tasks):
+            if last:
+                mixed = total[i][:HEAD_DIM] / total[i][HEAD_DIM : HEAD_DIM + 1]
+                mixed = mixed.T.astype(BF16)
+                here = pl.ds(pl.multiple_of(b * WINDOW_REACH, WINDOW_REACH), WINDOW_REACH)
+                for n, k in enumerate(query_heads(h)):
+                    attended[here, k * HEAD_DIM : (k + 1) * HEAD_DIM] = mixed[
+                        n * WINDOW_REACH : (n + 1) * WINDOW_REACH
+                    ]
+            else:
+                sums[b, h] = total[i]
+                tops[b, h, 0:1, :] = top[i]
+
+    def attend_all(n, first_block, pieces, most, **kind):
+        each = max(i for i in range(1, most + 1) if n % i == 0)
+        loop(
+            0,
+            n // each,
+            lambda g: attend([(first_block + g * each + i, pieces) for i in range(each)], **kind),
+        )
+
+    def start_block(b):
+        for h in range(kv_local):
+            sums[b, h, :HEAD_DIM, :] = jnp.zeros((HEAD_DIM, stacked), F32)
+            sums[b, h, HEAD_DIM:, :] = jnp.ones((8, stacked), F32)
+            tops[b, h, 0:1, :] = sinks(h)
+
+    def opposite_arrived(base):
+        for half in range(2):
+            ctx_copy(base + opposite, sp, 0, half).wait_recv()
+
+    def transpose_chunk(piece):
+        values = ctx_kv[pl.ds(piece * slots_each, slots_each), :, pl.ds(pair, pair)]
+        at = pl.multiple_of(piece * chunk_rows, chunk_rows)
+        ctx_values_t[:, pl.ds(at, chunk_rows)] = values.reshape(chunk_rows, pair).T
+
+    def receive_chunk(k):
+        if lines_each == 1:
+            opposite_arrived(line_base(k))
+        elif k == 0:
+            loop(0, lines, lambda i: opposite_arrived(i * QUAD))
+        transpose_chunk(chunk_at(k))
+
+    early = aligned and n_tp == 2 and blocks >= 6
+    inner = blocks - 2
+
+    project_kv(WINDOW_REACH + tp * rows)
+    loop(1, n_tp, lambda d: hid_copy(d, False).wait_recv())
+    loop(1, n_tp, lambda d: project_kv(WINDOW_REACH + lax.rem(tp + d, n_tp) * rows))
+    transpose_values()
+    serve(0)
     loads[7].wait()
     project_q(tp)
+    serve(1)
+    loop(1, n_tp, lambda d: project_q(lax.rem(tp + d, n_tp)))
+    if early:
+        attend_all(inner, 1, [WINDOW], 2, first=True)
+        start_block(0)
+        start_block(blocks - 1)
+    else:
+        loop(0, blocks, start_block)
     serve(2)
-    loop(1, n_tp, lambda d: project_q(lax.rem(tp + d, n_tp)))
-    if raw_halo:
-
-        @pl.when(has_last & holds_last)
-        def _():
-            receive_edge(True)
-
-        @pl.when(has_next & holds_first)
-        def _():
-            receive_edge(False)
-
-        @pl.when(jnp.logical_not(has_last))
-        def _():
-            hidden[0:WINDOW_REACH, :] = jnp.zeros((WINDOW_REACH, width), BF16)
-
-        @pl.when(jnp.logical_not(has_next))
-        def _():
-            hidden[WINDOW_REACH + group_rows :, :] = jnp.zeros((WINDOW_REACH, width), BF16)
-
-    for step in range(3, lines):
-        serve(step)
-    if raw_halo:
-
-        @pl.when(has_last & jnp.logical_not(holds_last))
-        def _():
-            edge_copy(True, 0, False).wait_recv()
-
-        @pl.when(has_next & jnp.logical_not(holds_first))
-        def _():
-            edge_copy(False, 0, False).wait_recv()
-
-        project_kv(0, WINDOW_REACH)
-        project_kv(WINDOW_REACH + group_rows, WINDOW_REACH)
-    else:
-
-        @pl.when(has_last)
-        def _():
-            halo_copy(True).wait_recv()
-
-        @pl.when(has_next)
-        def _():
-            halo_copy(False).wait_recv()
-
-    def opposite_arrivals(i):
-        slot = i * QUAD + opposite
-        ctx_copy(slot, sp, 0, 0).wait_recv()
-        ctx_copy(slot, sp, 0, 1).wait_recv()
-
-    loop(0, lines, opposite_arrivals)
-
-    span = 3 * WINDOW_REACH
-    stacked = per_group * WINDOW_REACH
-    total_rows = group_rows * n_sp
-    ctx_total = n_sp * ctx_rows
-    contract = (((1,), (1,)), ((), ()))
-
-    def attend(block):
-        begin = pl.multiple_of(block * WINDOW_REACH, WINDOW_REACH)
-        here = pl.ds(begin, WINDOW_REACH)
-        around = pl.ds(begin, span)
-        query_at = lax.rem(
-            lax.broadcasted_iota(jnp.int32, (stacked, span), 0), WINDOW_REACH
-        ) + WINDOW_REACH
-        key_at = lax.broadcasted_iota(jnp.int32, (stacked, span), 1)
-        key_pos = sp * group_rows + begin - WINDOW_REACH + key_at
-        allowed = (
-            (jnp.abs(key_at - query_at) <= WINDOW_REACH) & (key_pos >= 0) & (key_pos < total_rows)
-        )
-        for h in range(kv_local):
-            heads = [h * per_group + i for i in range(per_group)]
-            cols = slice(h * HEAD_DIM, (h + 1) * HEAD_DIM)
-            value_cols = slice(pair + h * HEAD_DIM, pair + (h + 1) * HEAD_DIM)
-            q = jnp.concatenate(
-                [queries[here, i * HEAD_DIM : (i + 1) * HEAD_DIM] for i in heads], axis=0
-            )
-            band = lax.dot_general(q, kv[around, cols], contract, preferred_element_type=F32)
-            band = jnp.where(allowed, band, MASKED_SCORE)
-            ctx_keys = ctx_kv[:, :, cols].reshape(ctx_total, HEAD_DIM)
-            ctx_values = ctx_kv[:, :, value_cols].reshape(ctx_total, HEAD_DIM)
-            far = lax.dot_general(q, ctx_keys, contract, preferred_element_type=F32)
-            sink = jnp.concatenate(
-                [jnp.full((WINDOW_REACH, 1), sink_ref[0, i] * log2e, F32) for i in heads], axis=0
-            )
-            top = jnp.maximum(
-                jnp.maximum(
-                    jnp.max(band, axis=-1, keepdims=True), jnp.max(far, axis=-1, keepdims=True)
-                ),
-                sink,
-            )
-            band_exp = jnp.exp2(band - top)
-            far_exp = jnp.exp2(far - top)
-            total = (
-                jnp.sum(band_exp, axis=-1, keepdims=True)
-                + jnp.sum(far_exp, axis=-1, keepdims=True)
-                + jnp.exp2(sink - top)
-            )
-            mixed = jnp.dot(
-                band_exp.astype(BF16), kv[around, value_cols], preferred_element_type=F32
-            ) + jnp.dot(far_exp.astype(BF16), ctx_values, preferred_element_type=F32)
-            mixed = (mixed / total).astype(BF16)
-            for n, i in enumerate(heads):
-                attended[here, i * HEAD_DIM : (i + 1) * HEAD_DIM] = mixed[
-                    n * WINDOW_REACH : (n + 1) * WINDOW_REACH
-                ]
-
-    by_part = rows % WINDOW_REACH == 0
+    send_halo()
+    if lines_each > 1:
+        for step in range(3, lines):
+            serve(step)
+    receive_chunk(0)
+    attend_all(blocks, 0, [chunk_at(0)], 3)
+    if lines_each == 1:
+        for step in range(3, lines):
+            serve(step)
+    for k in range(1, ctx_chunks - 1):
+        receive_chunk(k)
+        attend_all(blocks, 0, [chunk_at(k)], 3)
+    receive_chunk(ctx_chunks - 1)
+    receive_halo()
+    final = chunk_at(ctx_chunks - 1)
+
     part_blocks = rows // WINDOW_REACH
 
-    def attend_part(slot):
-        if by_part:
-            loop(0, part_blocks, lambda b: attend(slot * part_blocks + b))
-
-    if not by_part:
-        loop(0, group_rows // WINDOW_REACH, attend)
+    def finish_part(slot):
+        if early:
+            edge = slot * (blocks - 1)
+            from_block = slot * part_blocks + 1 - slot
+            inside = [(from_block + i, [final]) for i in range(part_blocks - 1)]
+            attend(inside + [(edge, [final, WINDOW])], last=True)
+
+    if not early:
+        attend_all(blocks, 0, [final, WINDOW], 2, last=True)
     loads[8].wait()
     out_tile = tile_of(width, 512)
 
@@ -647,7 +689,7 @@
 
     def peer_part(d):
         slot = lax.rem(tp + d, n_tp)
-        attend_part(slot)
+        finish_part(slot)
 
         def store(cols, value):
             partial_out[slot, :, cols] = value
@@ -656,7 +698,7 @@
         out_copy(d, True).start()
 
     loop(1, n_tp, peer_part)
-    attend_part(tp)
+    finish_part(tp)
 
     def keep(cols, value):
         own_total[:, cols] = value.astype(F32)
@@ -680,34 +722,15 @@
     for copy in ctx_sends:
         copy.wait_send()
 
-    if raw_halo:
-
-        @pl.when(has_next & holds_last)
-        def _():
-            raw_copy(True, 0).wait_send()
-            raw_copy(True, 1).wait_send()
-
-        @pl.when(has_last & holds_first)
-        def _():
-            raw_copy(False, 0).wait_send()
-            raw_copy(False, 1).wait_send()
-
-        @pl.when(has_last & holds_last)
-        def _():
-            loop(1, n_tp, lambda d: edge_copy(True, d, True).wait_send())
-
-        @pl.when(has_next & holds_first)
-        def _():
-            loop(1, n_tp, lambda d: edge_copy(False, d, True).wait_send())
-    else:
-
-        @pl.when(has_next)
-        def _():
-            halo_copy(True).wait_send()
-
-        @pl.when(has_last)
-        def _():
-            halo_copy(False).wait_send()
+    @pl.when(has_next)
+    def _():
+        for copy in halo_copies(True):
+            copy.wait_send()
+
+    @pl.when(has_last)
+    def _():
+        for copy in halo_copies(False):
+            copy.wait_send()
 
 
 def angle_tables(total_rows):
@@ -757,6 +780,9 @@
     ctx_rows = context.shape[0]
     lines = n_sp // QUAD
     ctx_sends = (lines - 1) + 4 * lines
+    padded = group_rows + 2 * WINDOW_REACH
+    state = (group_rows // WINDOW_REACH, pair // HEAD_DIM)
+    stacked = query_width // pair * WINDOW_REACH
     dma = pltpu.SemaphoreType.DMA
     vmem = pl.BlockSpec(memory_space=pltpu.VMEM)
     anywhere = pl.BlockSpec(memory_space=pl.ANY)
@@ -786,15 +812,19 @@
             pltpu.VMEM((group_rows + 2 * WINDOW_REACH, width), BF16),
             like(context),
             pltpu.VMEM((group_rows, query_width), BF16),
-            pltpu.VMEM((group_rows + 2 * WINDOW_REACH, 2 * pair), BF16),
+            pltpu.VMEM((padded, pair), BF16),
+            pltpu.VMEM((8 if rows % WINDOW_REACH == 0 else padded, pair), BF16),
+            pltpu.VMEM((pair, padded), BF16),
             pltpu.VMEM((n_sp, ctx_rows, 2 * pair), BF16),
+            pltpu.VMEM((pair, n_sp * ctx_rows), BF16),
+            pltpu.VMEM((*state, HEAD_DIM + 8, stacked), F32),
+            pltpu.VMEM((*state, 8, stacked), F32),
             pltpu.VMEM((group_rows, query_width), BF16),
             pltpu.VMEM((n_tp, rows, width), BF16),
             pltpu.VMEM((n_tp, rows, width), BF16),
             pltpu.VMEM((rows, width), F32),
             pltpu.VMEM((group_rows + 2 * WINDOW_REACH, HEAD_DIM), F32),
             pltpu.VMEM((group_rows + 2 * WINDOW_REACH, HEAD_DIM), F32),
-            pltpu.VMEM((2, WINDOW_REACH, width), BF16),
             dma((9,)),
             dma((n_sp,)),
             dma((n_sp,)),
@@ -804,12 +834,8 @@
             dma((n_tp,)),
             dma((ctx_sends,)),
             dma((n_sp, 2)),
-            dma((2,)),
-            dma((2,)),
             dma((2, 2)),
             dma((2, 2)),
-            dma((2, n_tp)),
-            dma((2,)),
             dma((n_tp,)),
             dma((n_tp,)),
         ],

time: 76.3 us -> 67.6 us (0.89)
  the two profiles are of different devices: /device:TPU:16 before, /device:TPU:0 now
where the time goes in v2:
time: 67.6 us; the launch traced here: 67.4 us
  Pallas kernels  64.7 us (96%)
  local copies, waits for them, and re-layouts  2.73 us (4%)
    pallas_call x1, Pallas kernels, shards(): pl.pallas_call(functools.partial(block_kernel, n_sp, n_tp), out_shape=jax...  64.7 us
    unnamed x1, local copies, waits for them, and re-layouts  2.73 us

profile of v2, /device:TPU:0, one launch (start us, length us, event | category | flops | bytes accessed | tf_op | source)
XLA Modules:
  0.0 67.4 jit_solution(5659696661068679248)
XLA Ops:
  0.0 64.7 %shard_map.163 = bf16[384,2048]{1,0:T(8,128)(2,1)} custom-call(f32[1,128]{1,0:T(1,128)} %bitcast.5, f32[1,128]{1,0:T(1,128)} %bitcast.6, f32[1,2048]{1,0:T(1,128)} %bitcast.4, f32[192,128]{1,0:T(8,128)} %constant.8.clone.row_cos, f32[192,128]{1,0:T(8,128)} %constant.9.clone.row_sin, f32[64,128]{1,0:T(8,128)} %constant.10.clone.col_cos, ...), custom_call_target="tpu_custom_call" | custom-call | tf_op jit(solution)/shard_map/pallas_call | solution.py:793
  64.7 2.7 %copy.19 = bf16[384,2048]{1,0:T(8,128)(2,1)} copy(bf16[384,2048]{1,0:T(8,128)(2,1)} %shard_map.163) | data formatting | bytes 3145728

commit v3 on v2

--- a/solution.py
+++ b/solution.py
@@ -79,6 +79,8 @@
     own_total,
     cos_ref,
     sin_ref,
+    halo_raw,
+    edge_hidden,
     load_sem,
     rs_send,
     rs_recv,
@@ -90,6 +92,8 @@
     ctx_recv,
     halo_send,
     halo_recv,
+    edge_send,
+    edge_recv,
     out_send,
     out_recv,
 ):
@@ -198,10 +202,38 @@
         lax.fori_loop(low, high, step, 0)
 
     has_next, has_last = sp < n_sp - 1, sp > 0
+    holds_last, holds_first = tp == n_tp - 1, tp == 0
+    raw_halo = rows >= WINDOW_REACH
+    half_reach = WINDOW_REACH // 2
+
+    def raw_copy(up, half):
+        which = 0 if up else 1
+        base = rows - WINDOW_REACH if up else 0
+        return pltpu.make_async_remote_copy(
+            src_ref=latent.at[pl.ds(base + half * half_reach, half_reach)],
+            dst_ref=halo_raw.at[which, pl.ds(half * half_reach, half_reach)],
+            send_sem=halo_send.at[which, half],
+            recv_sem=halo_recv.at[which, half],
+            device_id={"sp": lax.rem(sp + (1 if up else n_sp - 1), n_sp)},
+            device_id_type=MESH,
+        )
+
+    def send_raw(half):
+        if raw_halo:
+
+            @pl.when(has_next & holds_last)
+            def _():
+                raw_copy(True, half).start()
+
+            @pl.when(has_last & holds_first)
+            def _():
+                raw_copy(False, half).start()
 
     loop(1, n_sp, lambda d: rs_copy(d).start())
     gathered[sp] = part[sp]
     loads[4].wait()
+    loop(1, n_sp, lambda d: rs_copy(d).wait_send())
+    send_raw(0)
 
     strip = 32
 
@@ -251,6 +283,8 @@
         )
 
     loop(1, everyone, lambda d: ag_copy(d).start())
+    loop(1, everyone, lambda d: ag_copy(d).wait_send())
+    send_raw(1)
 
     loop(1, everyone, lambda d: ag_arrival(d).wait_recv())
 
@@ -334,11 +368,16 @@
         ctx_copy(line_base(d) + beside, sp, 0).wait_recv()
         send_ctx(line_base(d) + beside, line * QUAD + across, 1)
 
-    def serve(step):
-        if step < lines:
-            if step + 1 < lines:
-                forward(step + 1)
-            relay(step)
+    gather_steps = []
+    for d in range(lines):
+        if d + 1 < lines:
+            gather_steps.append(functools.partial(forward, d + 1))
+        gather_steps.append(functools.partial(relay, d))
+
+    def serve(count):
+        for step in gather_steps[:count]:
+            step()
+        del gather_steps[:count]
 
     own_start = pl.multiple_of(WINDOW_REACH + tp * rows, strip)
 
@@ -406,7 +445,7 @@
 
             loop(0, group_rows // WINDOW_REACH, one)
 
-    def project_q(slot):
+    def project_q(slot, begin=0, end=None):
         target = pl.ds(pl.multiple_of(slot * rows, strip), rows)
         source = pl.ds(pl.multiple_of(WINDOW_REACH + slot * rows, strip), rows)
         q_tile = tile_of(query_width, 512)
@@ -418,7 +457,8 @@
                 q * factor, cos_ref[source, :], sin_ref[source, :]
             )
 
-        loop(0, query_width // q_tile, one)
+        count = query_width // q_tile
+        loop(begin * count // 2, (2 if end is None else end) * count // 2, one)
 
     log2e = 1.4426950408889634
     factor = HEAD_DIM ** (-0.5) * log2e
@@ -447,6 +487,9 @@
         ]
 
     def send_halo():
+        if raw_halo:
+            return
+
         @pl.when(has_next)
         def _():
             for copy in halo_copies(True):
@@ -470,7 +513,81 @@
         def _():
             clear(group_rows + WINDOW_REACH)
 
+    def edge_copy(low, d, mine):
+        peer = lax.rem(tp + d, n_tp) if mine else tp
+        which = 0 if low else 1
+        region = pl.ds(which * WINDOW_REACH, WINDOW_REACH)
+        return pltpu.make_async_remote_copy(
+            src_ref=edge_hidden.at[region],
+            dst_ref=edge_hidden.at[region],
+            send_sem=edge_send.at[which, peer],
+            recv_sem=edge_recv.at[which],
+            device_id={"tp": peer},
+            device_id_type=MESH,
+        )
+
+    def scale_edge(low):
+        which = 0 if low else 1
+        raw_copy(low, 0).wait_recv()
+        raw_copy(low, 1).wait_recv()
+
+        def one(i):
+            at = pl.multiple_of(i * strip, strip)
+            edge_hidden[pl.ds(which * WINDOW_REACH + at, strip), :] = normed(
+                halo_raw[which, pl.ds(at, strip), :], 0, 2
+            )
+
+        loop(0, WINDOW_REACH // strip, one)
+        loop(1, n_tp, lambda d: edge_copy(low, d, True).start())
+
+    def scale_edges():
+        if not raw_halo:
+            return
+
+        @pl.when(has_last & holds_last)
+        def _():
+            scale_edge(True)
+
+        @pl.when(has_next & holds_first)
+        def _():
+            scale_edge(False)
+
+        @pl.when(jnp.logical_not(has_last))
+        def _():
+            edge_hidden[:WINDOW_REACH, :] = jnp.zeros((WINDOW_REACH, width), BF16)
+
+        @pl.when(jnp.logical_not(has_next))
+        def _():
+            edge_hidden[WINDOW_REACH:, :] = jnp.zeros((WINDOW_REACH, width), BF16)
+
+    def project_edges():
+        if not raw_halo:
+            return
+
+        @pl.when(has_last & jnp.logical_not(holds_last))
+        def _():
+            edge_copy(True, 0, False).wait_recv()
+
+        @pl.when(has_next & jnp.logical_not(holds_first))
+        def _():
+            edge_copy(False, 0, False).wait_recv()
+
+        def one(j):
+            col = pl.multiple_of(j * tile, tile)
+            keys = jnp.dot(edge_hidden[...], wk[:, pl.ds(col, tile)], preferred_element_type=F32)
+            values = jnp.dot(edge_hidden[...], wv[:, pl.ds(col, tile)], preferred_element_type=F32)
+            for which, start in enumerate((0, WINDOW_REACH + group_rows)):
+                part = slice(which * WINDOW_REACH, (which + 1) * WINDOW_REACH)
+                at = pl.ds(start, WINDOW_REACH)
+                keys_kept[at, pl.ds(col, tile)] = turned(keys[part], cos_ref[at, :], sin_ref[at, :])
+                values_t[pl.ds(col, tile), at] = values[part].astype(BF16).T
+
+        loop(0, pair // tile, one)
+
     def receive_halo():
+        if raw_halo:
+            return
+
         @pl.when(has_last)
         def _():
             for copy in halo_copies(True):
@@ -617,34 +734,36 @@
     early = aligned and n_tp == 2 and blocks >= 6
     inner = blocks - 2
 
+    loads[7].wait()
     project_kv(WINDOW_REACH + tp * rows)
+    project_q(tp)
     loop(1, n_tp, lambda d: hid_copy(d, False).wait_recv())
+    serve(2)
     loop(1, n_tp, lambda d: project_kv(WINDOW_REACH + lax.rem(tp + d, n_tp) * rows))
     transpose_values()
-    serve(0)
-    loads[7].wait()
-    project_q(tp)
-    serve(1)
-    loop(1, n_tp, lambda d: project_q(lax.rem(tp + d, n_tp)))
+    send_halo()
     if early:
+        project_q(1 - tp, 0, 1)
+        serve(1)
+        project_q(1 - tp, 1, 2)
+        serve(1)
         attend_all(inner, 1, [WINDOW], 2, first=True)
         start_block(0)
         start_block(blocks - 1)
+        serve(2)
     else:
+        loop(1, n_tp, lambda d: project_q(lax.rem(tp + d, n_tp)))
         loop(0, blocks, start_block)
-    serve(2)
-    send_halo()
     if lines_each > 1:
-        for step in range(3, lines):
-            serve(step)
+        serve(len(gather_steps))
     receive_chunk(0)
     attend_all(blocks, 0, [chunk_at(0)], 3)
-    if lines_each == 1:
-        for step in range(3, lines):
-            serve(step)
+    serve(len(gather_steps))
+    scale_edges()
     for k in range(1, ctx_chunks - 1):
         receive_chunk(k)
         attend_all(blocks, 0, [chunk_at(k)], 3)
+    project_edges()
     receive_chunk(ctx_chunks - 1)
     receive_halo()
     final = chunk_at(ctx_chunks - 1)
@@ -715,22 +834,41 @@
 
     loop(0, rows // strip, finish)
 
-    loop(1, n_sp, lambda d: rs_copy(d).wait_send())
-    loop(1, everyone, lambda d: ag_copy(d).wait_send())
     loop(1, n_tp, lambda d: hid_copy(d, True).wait_send())
     loop(1, n_tp, lambda d: out_copy(d, True).wait_send())
     for copy in ctx_sends:
         copy.wait_send()
 
-    @pl.when(has_next)
-    def _():
-        for copy in halo_copies(True):
-            copy.wait_send()
-
-    @pl.when(has_last)
-    def _():
-        for copy in halo_copies(False):
-            copy.wait_send()
+    if raw_halo:
+
+        @pl.when(has_next & holds_last)
+        def _():
+            raw_copy(True, 0).wait_send()
+            raw_copy(True, 1).wait_send()
+
+        @pl.when(has_last & holds_first)
+        def _():
+            raw_copy(False, 0).wait_send()
+            raw_copy(False, 1).wait_send()
+
+        @pl.when(has_last & holds_last)
+        def _():
+            loop(1, n_tp, lambda d: edge_copy(True, d, True).wait_send())
+
+        @pl.when(has_next & holds_first)
+        def _():
+            loop(1, n_tp, lambda d: edge_copy(False, d, True).wait_send())
+    else:
+
+        @pl.when(has_next)
+        def _():
+            for copy in halo_copies(True):
+                copy.wait_send()
+
+        @pl.when(has_last)
+        def _():
+            for copy in halo_copies(False):
+                copy.wait_send()
 
 
 def angle_tables(total_rows):
@@ -809,7 +947,7 @@
             pltpu.VMEM((n_sp, per, LANES), F32),
             pltpu.VMEM((n_tp, n_sp, per, LANES), F32),
             pltpu.VMEM((8, width), F32),
-            pltpu.VMEM((group_rows + 2 * WINDOW_REACH, width), BF16),
+            pltpu.VMEM((padded, width), BF16),
             like(context),
             pltpu.VMEM((group_rows, query_width), BF16),
             pltpu.VMEM((padded, pair), BF16),
@@ -825,6 +963,8 @@
             pltpu.VMEM((rows, width), F32),
             pltpu.VMEM((group_rows + 2 * WINDOW_REACH, HEAD_DIM), F32),
             pltpu.VMEM((group_rows + 2 * WINDOW_REACH, HEAD_DIM), F32),
+            pltpu.VMEM((2, WINDOW_REACH, width), BF16),
+            pltpu.VMEM((2 * WINDOW_REACH, width), BF16),
             dma((9,)),
             dma((n_sp,)),
             dma((n_sp,)),
@@ -836,6 +976,8 @@
             dma((n_sp, 2)),
             dma((2, 2)),
             dma((2, 2)),
+            dma((2, n_tp)),
+            dma((2,)),
             dma((n_tp,)),
             dma((n_tp,)),
         ],

time: 67.6 us -> 64.5 us (0.954)
  the two profiles are of different devices: /device:TPU:0 before, /device:TPU:16 now
where the time goes in v3:
time: 64.5 us; the launch traced here: 64.4 us
  Pallas kernels  61.6 us (96%)
  local copies, waits for them, and re-layouts  2.73 us (4%)
    pallas_call x1, Pallas kernels, shards(): pl.pallas_call(functools.partial(block_kernel, n_sp, n_tp), out_shape=jax...  61.6 us
    unnamed x1, local copies, waits for them, and re-layouts  2.73 us

profile of v3, /device:TPU:16, one launch (start us, length us, event | category | flops | bytes accessed | tf_op | source)
XLA Modules:
  0.0 64.4 jit_solution(2192805348988902585)
XLA Ops:
  0.0 61.6 %shard_map.163 = bf16[384,2048]{1,0:T(8,128)(2,1)} custom-call(f32[1,128]{1,0:T(1,128)} %bitcast.5, f32[1,128]{1,0:T(1,128)} %bitcast.6, f32[1,2048]{1,0:T(1,128)} %bitcast.4, f32[192,128]{1,0:T(8,128)} %constant.8.clone.row_cos, f32[192,128]{1,0:T(8,128)} %constant.9.clone.row_sin, f32[64,128]{1,0:T(8,128)} %constant.10.clone.col_cos, ...), custom_call_target="tpu_custom_call" | custom-call | tf_op jit(solution)/shard_map/pallas_call | solution.py:931
  61.6 2.7 %copy.19 = bf16[384,2048]{1,0:T(8,128)(2,1)} copy(bf16[384,2048]{1,0:T(8,128)(2,1)} %shard_map.163) | data formatting | bytes 3145728

commit v4 on v3

--- a/solution.py
+++ b/solution.py
@@ -60,8 +60,8 @@
     wv,
     wo,
     part,
-    gathered,
-    full,
+    line_parts,
+    quad_parts,
     mod,
     hidden,
     ctx_hidden,
@@ -82,10 +82,10 @@
     halo_raw,
     edge_hidden,
     load_sem,
-    rs_send,
-    rs_recv,
-    ag_send,
-    ag_recv,
+    line_send,
+    line_recv,
+    quad_send,
+    quad_recv,
     hid_send,
     hid_recv,
     ctx_send,
@@ -103,7 +103,6 @@
     group_rows = rows * n_tp
     columns = shift_w.shape[1]
     chunks = columns // LANES
-    per = part.shape[1]
     query_width = wq.shape[1]
     pair = wk.shape[1]
     kv_local = pair // HEAD_DIM
@@ -131,21 +130,33 @@
 
     barrier = pltpu.get_barrier_semaphore()
 
-    everyone = n_sp * n_tp
-    me = sp * n_tp + tp
-
-    def other(d):
-        at = lax.rem(me + d, everyone)
-        return at // n_tp, lax.rem(at, n_tp)
-
-    def greet(d, carry):
-        peer_sp, peer_tp = other(d)
-        pl.semaphore_signal(
-            barrier, inc=1, device_id={"sp": peer_sp, "tp": peer_tp}, device_id_type=MESH
-        )
-        return carry
-
-    lax.fori_loop(1, everyone, greet, 0)
+    lines = n_sp // QUAD
+    line, corner = sp // QUAD, lax.rem(sp, QUAD)
+    cluster = QUAD * n_tp
+
+    def loop(low, high, f):
+        def step(i, carry):
+            f(i)
+            return carry
+
+        lax.fori_loop(low, high, step, 0)
+
+    def in_line(d):
+        peer = lax.rem(line + d, lines)
+        return peer, {"sp": peer * QUAD + corner}
+
+    def in_cluster(d):
+        at = lax.rem(corner * n_tp + tp + d, cluster)
+        peer, peer_tp = at // n_tp, lax.rem(at, n_tp)
+        return peer, peer_tp, {"sp": line * QUAD + peer, "tp": peer_tp}
+
+    def greet(device):
+        pl.semaphore_signal(barrier, inc=1, device_id=device, device_id_type=MESH)
+
+    loop(1, lines, lambda d: greet(in_line(d)[1]))
+    loop(1, cluster, lambda d: greet(in_cluster(d)[2]))
+    for d in (1, n_sp - 1):
+        greet({"sp": lax.rem(sp + d, n_sp)})
 
     def silu(v):
         return v / (1.0 + jnp.exp(-v))
@@ -165,74 +176,60 @@
         for v in range(count):
             for j in range(chunks):
                 g = vector * chunks + j
-                part[g // per, g % per : g % per + 1, :] = product[
+                part[g : g + 1, :] = product[
                     v : v + 1, j * LANES : (j + 1) * LANES
                 ]
             vector += 1
 
-    pl.semaphore_wait(barrier, everyone - 1)
-
-    def rs_copy(d):
-        peer = lax.rem(sp + d, n_sp)
+    pl.semaphore_wait(barrier, lines + cluster)
+
+    def line_copy(d, mine):
+        peer, device = in_line(d)
+        slot = line if mine else peer
         return pltpu.make_async_remote_copy(
-            src_ref=part.at[peer],
-            dst_ref=gathered.at[sp],
-            send_sem=rs_send.at[peer],
-            recv_sem=rs_recv.at[sp],
-            device_id={"sp": peer},
+            src_ref=part,
+            dst_ref=line_parts.at[slot],
+            send_sem=line_send.at[peer],
+            recv_sem=line_recv.at[slot],
+            device_id=device,
             device_id_type=MESH,
         )
-
-    def rs_arrival(d):
-        peer = lax.rem(sp + d, n_sp)
-        return pltpu.make_async_remote_copy(
-            src_ref=part.at[peer],
-            dst_ref=gathered.at[peer],
-            send_sem=rs_send.at[peer],
-            recv_sem=rs_recv.at[peer],
-            device_id={"sp": peer},
-            device_id_type=MESH,
-        )
-
-    def loop(low, high, f):
-        def step(i, carry):
-            f(i)
-            return carry
-
-        lax.fori_loop(low, high, step, 0)
 
     has_next, has_last = sp < n_sp - 1, sp > 0
     holds_last, holds_first = tp == n_tp - 1, tp == 0
     raw_halo = rows >= WINDOW_REACH
-    half_reach = WINDOW_REACH // 2
-
-    def raw_copy(up, half):
+    raw_ends = (0, 0, 128, 128)
+
+    def raw_copy(up, piece):
         which = 0 if up else 1
         base = rows - WINDOW_REACH if up else 0
+        begin, count = raw_ends[piece], raw_ends[piece + 1] - raw_ends[piece]
         return pltpu.make_async_remote_copy(
-            src_ref=latent.at[pl.ds(base + half * half_reach, half_reach)],
-            dst_ref=halo_raw.at[which, pl.ds(half * half_reach, half_reach)],
-            send_sem=halo_send.at[which, half],
-            recv_sem=halo_recv.at[which, half],
+            src_ref=latent.at[pl.ds(base + begin, count)],
+            dst_ref=halo_raw.at[which, pl.ds(begin, count)],
+            send_sem=halo_send.at[which, piece],
+            recv_sem=halo_recv.at[which, piece],
             device_id={"sp": lax.rem(sp + (1 if up else n_sp - 1), n_sp)},
             device_id_type=MESH,
         )
 
-    def send_raw(half):
-        if raw_halo:
+    raw_pieces = [i for i in range(3) if raw_ends[i + 1] > raw_ends[i]]
+
+    def send_raw(piece):
+        if raw_halo and piece in raw_pieces:
 
             @pl.when(has_next & holds_last)
             def _():
-                raw_copy(True, half).start()
+                raw_copy(True, piece).start()
 
             @pl.when(has_last & holds_first)
             def _():
-                raw_copy(False, half).start()
-
-    loop(1, n_sp, lambda d: rs_copy(d).start())
-    gathered[sp] = part[sp]
+                raw_copy(False, piece).start()
+
+    loop(1, lines, lambda d: line_copy(d, True).start())
+    line_parts[line] = part[...]
     loads[4].wait()
-    loop(1, n_sp, lambda d: rs_copy(d).wait_send())
+    loop(1, lines, lambda d: line_copy(d, True).wait_send())
     send_raw(0)
 
     strip = 32
@@ -257,43 +254,32 @@
             target[at, :] = jnp.where(in_row, spread, by_col[...])
 
     loop(0, grid_rows + 2 * grid_pad, fill_angles)
-    loop(1, n_sp, lambda d: rs_arrival(d).wait_recv())
-    full[tp, sp] = jnp.sum(gathered[...], axis=0)
-
-    def ag_copy(d):
-        peer_sp, peer_tp = other(d)
+    loop(1, lines, lambda d: line_copy(d, False).wait_recv())
+    quad_parts[tp, corner] = jnp.sum(line_parts[...], axis=0)
+
+    def quad_copy(d, mine):
+        peer, peer_tp, device = in_cluster(d)
+        at = (tp, corner) if mine else (peer_tp, peer)
         return pltpu.make_async_remote_copy(
-            src_ref=full.at[tp, sp],
-            dst_ref=full.at[tp, sp],
-            send_sem=ag_send.at[peer_tp, peer_sp],
-            recv_sem=ag_recv.at[tp, sp],
-            device_id={"sp": peer_sp, "tp": peer_tp},
+            src_ref=quad_parts.at[tp, corner],
+            dst_ref=quad_parts.at[at],
+            send_sem=quad_send.at[peer_tp, peer],
+            recv_sem=quad_recv.at[at],
+            device_id=device,
             device_id_type=MESH,
         )
 
-    def ag_arrival(d):
-        peer_sp, peer_tp = other(d)
-        return pltpu.make_async_remote_copy(
-            src_ref=full.at[tp, sp],
-            dst_ref=full.at[peer_tp, peer_sp],
-            send_sem=ag_send.at[peer_tp, peer_sp],
-            recv_sem=ag_recv.at[peer_tp, peer_sp],
-            device_id={"sp": peer_sp, "tp": peer_tp},
-            device_id_type=MESH,
-        )
-
-    loop(1, everyone, lambda d: ag_copy(d).start())
-    loop(1, everyone, lambda d: ag_copy(d).wait_send())
+    loop(1, cluster, lambda d: quad_copy(d, True).start())
+    loop(1, cluster, lambda d: quad_copy(d, True).wait_send())
     send_raw(1)
-
-    loop(1, everyone, lambda d: ag_arrival(d).wait_recv())
-
+    loop(1, cluster, lambda d: quad_copy(d, False).wait_recv())
     for t in range(n_tp):
+        whole = jnp.sum(quad_parts[t], axis=0)
         for v in range(5):
             for j in range(chunks):
                 g = v * chunks + j
                 column = t * columns + j * LANES
-                mod[v : v + 1, column : column + LANES] = full[t, g // per, g % per : g % per + 1, :]
+                mod[v : v + 1, column : column + LANES] = whole[g : g + 1, :]
     gain = gain_ref[...]
     mod[2:3, :] = gain * (1.0 + mod[2:3, :])
     mod[3:4, :] = gain * (1.0 + mod[3:4, :])
@@ -320,9 +306,6 @@
         ).astype(BF16)
 
     loop(0, pair // tile, ctx_project)
-
-    lines = n_sp // QUAD
-    line, corner = sp // QUAD, lax.rem(sp, QUAD)
 
     across = corner + 1 - 2 * lax.rem(corner, 2)
     beside = lax.rem(corner + 2, QUAD)
@@ -353,6 +336,7 @@
     for d in range(1, lines):
         send_ctx(sp, lax.rem(line + d, lines) * QUAD + corner)
     send_quad(sp)
+    send_raw(2)
 
     def line_base(d):
         return lax.rem(line + lines - d, lines) * QUAD
@@ -528,8 +512,8 @@
 
     def scale_edge(low):
         which = 0 if low else 1
-        raw_copy(low, 0).wait_recv()
-        raw_copy(low, 1).wait_recv()
+        for piece in raw_pieces:
+            raw_copy(low, piece).wait_recv()
 
         def one(i):
             at = pl.multiple_of(i * strip, strip)
@@ -780,7 +764,7 @@
     if not early:
         attend_all(blocks, 0, [final, WINDOW], 2, last=True)
     loads[8].wait()
-    out_tile = tile_of(width, 512)
+    out_tile = tile_of(width, 1024)
 
     def out_copy(d, mine):
         peer = lax.rem(tp + d, n_tp)
@@ -843,13 +827,13 @@
 
         @pl.when(has_next & holds_last)
         def _():
-            raw_copy(True, 0).wait_send()
-            raw_copy(True, 1).wait_send()
+            for piece in raw_pieces:
+                raw_copy(True, piece).wait_send()
 
         @pl.when(has_last & holds_first)
         def _():
-            raw_copy(False, 0).wait_send()
-            raw_copy(False, 1).wait_send()
+            for piece in raw_pieces:
+                raw_copy(False, piece).wait_send()
 
         @pl.when(has_last & holds_last)
         def _():
@@ -911,8 +895,7 @@
     group_rows = rows * n_tp
     angles = [jnp.asarray(t) for t in angle_tables(group_rows * n_sp)]
     columns = shift_weight.shape[1]
-    groups = 5 * columns // LANES
-    per = -(-groups // n_sp)
+    groups = -(-5 * columns // LANES // 8) * 8
     query_width = query_weight.shape[1]
     pair = key_matrix.shape[1]
     ctx_rows = context.shape[0]
@@ -943,9 +926,9 @@
             like(key_matrix),
             like(value_matrix),
             like(out_weight),
-            pltpu.VMEM((n_sp, per, LANES), F32),
-            pltpu.VMEM((n_sp, per, LANES), F32),
-            pltpu.VMEM((n_tp, n_sp, per, LANES), F32),
+            pltpu.VMEM((groups, LANES), F32),
+            pltpu.VMEM((lines, groups, LANES), F32),
+            pltpu.VMEM((n_tp, QUAD, groups, LANES), F32),
             pltpu.VMEM((8, width), F32),
             pltpu.VMEM((padded, width), BF16),
             like(context),
@@ -966,16 +949,16 @@
             pltpu.VMEM((2, WINDOW_REACH, width), BF16),
             pltpu.VMEM((2 * WINDOW_REACH, width), BF16),
             dma((9,)),
-            dma((n_sp,)),
-            dma((n_sp,)),
-            dma((n_tp, n_sp)),
-            dma((n_tp, n_sp)),
+            dma((lines,)),
+            dma((lines,)),
+            dma((n_tp, QUAD)),
+            dma((n_tp, QUAD)),
             dma((n_tp,)),
             dma((n_tp,)),
             dma((ctx_sends,)),
             dma((n_sp, 2)),
-            dma((2, 2)),
-            dma((2, 2)),
+            dma((2, 3)),
+            dma((2, 3)),
             dma((2, n_tp)),
             dma((2,)),
             dma((n_tp,)),

time: 64.5 us -> 62.2 us (0.964)
  Pallas kernels: 61.6 us -> 59.3 us
    pallas_call x1, Pallas kernels: 61.6 us -> 59.3 us  [shards(): pl.pallas_call(functools.partial(block_kernel, n_sp, n_tp), out_shape=jax...]
where the time goes in v4:
time: 62.2 us; the launch traced here: 62 us
  Pallas kernels  59.3 us (95%)
  local copies, waits for them, and re-layouts  2.73 us (4%)
    pallas_call x1, Pallas kernels, shards(): pl.pallas_call(functools.partial(block_kernel, n_sp, n_tp), out_shape=jax...  59.3 us
    unnamed x1, local copies, waits for them, and re-layouts  2.73 us

profile of v4, /device:TPU:16, one launch (start us, length us, event | category | flops | bytes accessed | tf_op | source)
XLA Modules:
  0.0 62.0 jit_solution(5124364703378358342)
XLA Ops:
  0.0 59.3 %shard_map.163 = bf16[384,2048]{1,0:T(8,128)(2,1)} custom-call(f32[1,128]{1,0:T(1,128)} %bitcast.5, f32[1,128]{1,0:T(1,128)} %bitcast.6, f32[1,2048]{1,0:T(1,128)} %bitcast.4, f32[192,128]{1,0:T(8,128)} %constant.8.clone.row_cos, f32[192,128]{1,0:T(8,128)} %constant.9.clone.row_sin, f32[64,128]{1,0:T(8,128)} %constant.10.clone.col_cos, ...), custom_call_target="tpu_custom_call" | custom-call | tf_op jit(solution)/shard_map/pallas_call | solution.py:914
  59.3 2.7 %copy.19 = bf16[384,2048]{1,0:T(8,128)(2,1)} copy(bf16[384,2048]{1,0:T(8,128)(2,1)} %shard_map.163) | data formatting | bytes 3145728

commit v5 on v4

--- a/solution.py
+++ b/solution.py
@@ -734,20 +734,21 @@
         attend_all(inner, 1, [WINDOW], 2, first=True)
         start_block(0)
         start_block(blocks - 1)
+        scale_edges()
         serve(2)
     else:
         loop(1, n_tp, lambda d: project_q(lax.rem(tp + d, n_tp)))
         loop(0, blocks, start_block)
+        scale_edges()
     if lines_each > 1:
         serve(len(gather_steps))
     receive_chunk(0)
     attend_all(blocks, 0, [chunk_at(0)], 3)
+    project_edges()
     serve(len(gather_steps))
-    scale_edges()
     for k in range(1, ctx_chunks - 1):
         receive_chunk(k)
         attend_all(blocks, 0, [chunk_at(k)], 3)
-    project_edges()
     receive_chunk(ctx_chunks - 1)
     receive_halo()
     final = chunk_at(ctx_chunks - 1)

time: 62.2 us -> 60.1 us (0.966)
  Pallas kernels: 59.3 us -> 57.2 us
    pallas_call x1, Pallas kernels: 59.3 us -> 57.2 us  [shards(): pl.pallas_call(functools.partial(block_kernel, n_sp, n_tp), out_shape=jax...]
where the time goes in v5:
time: 60.1 us; the launch traced here: 60 us
  Pallas kernels  57.2 us (95%)
  local copies, waits for them, and re-layouts  2.73 us (5%)
    pallas_call x1, Pallas kernels, shards(): pl.pallas_call(functools.partial(block_kernel, n_sp, n_tp), out_shape=jax...  57.2 us
    unnamed x1, local copies, waits for them, and re-layouts  2.73 us

profile of v5, /device:TPU:16, one launch (start us, length us, event | category | flops | bytes accessed | tf_op | source)
XLA Modules:
  0.0 60.0 jit_solution(15080869118061009066)
XLA Ops:
  0.0 57.2 %shard_map.163 = bf16[384,2048]{1,0:T(8,128)(2,1)} custom-call(f32[1,128]{1,0:T(1,128)} %bitcast.5, f32[1,128]{1,0:T(1,128)} %bitcast.6, f32[1,2048]{1,0:T(1,128)} %bitcast.4, f32[192,128]{1,0:T(8,128)} %constant.8.clone.row_cos, f32[192,128]{1,0:T(8,128)} %constant.9.clone.row_sin, f32[64,128]{1,0:T(8,128)} %constant.10.clone.col_cos, ...), custom_call_target="tpu_custom_call" | custom-call | tf_op jit(solution)/shard_map/pallas_call | solution.py:915
  57.2 2.7 %copy.19 = bf16[384,2048]{1,0:T(8,128)(2,1)} copy(bf16[384,2048]{1,0:T(8,128)(2,1)} %shard_map.163) | data formatting | bytes 3145728
